TPU v7x, 128 devices: a whole 4x4x4 slice. The times are simulated.
128 devices in a mesh: ep: 128 (over z, y, x, core).
Axes of the slice: x: 4, y: 4, z: 4, core: 2. Of those that a mesh axis runs over, the one named last changes fastest.
Arguments:
- residual: bfloat16 [8192, 2048], P('ep'), may hold values from -6 to 6
- branch_in: bfloat16 [8192, 1024], P('ep'), may hold values from -6 to 6
- state_real: float32 [8192, 4096], P('ep'), may hold values from -4 to 4
- state_imag: float32 [8192, 4096], P('ep'), may hold values from -4 to 4
- decay_rate: float32 [64, 64], replicated, may hold values from 0.1 to 1
- frequency: float32 [64, 64], replicated, may hold values from 0 to 200
- log_step: float32 [64], replicated, may hold values from -4 to 0
- input_real: bfloat16 [64, 64, 16], replicated, may hold values from -1 to 1
- input_imag: bfloat16 [64, 64, 16], replicated, may hold values from -1 to 1
- output_matrix_real: bfloat16 [64, 16, 64], replicated, may hold values from -0.5 to 0.5
- output_matrix_imaginary: bfloat16 [64, 16, 64], replicated, may hold values from -0.5 to 0.5
- skip_gain: float32 [1024], replicated, may hold values from -4 to 4
- glu_value: bfloat16 [1024, 2048], replicated, may hold values from -0.1875 to 0.1875
- glu_gate: bfloat16 [1024, 2048], replicated, may hold values from -0.1875 to 0.1875
- mix_gain: float32 [2048], replicated, may hold values from 0.1 to 1.9
- moe_in_gain: float32 [2048], replicated, may hold values from 0.1 to 1.9
- moe_out_gain: float32 [2048], replicated, may hold values from 0.1 to 1.9
- routes: int32 [8192, 6], P('ep'), may hold values from 0 to 127, all different within a row; in each aligned block of 64 rows (0 to 63, 64 to 127, ...) at most 4 rows name the same one
- route_weights: float32 [8192, 6], P('ep'), may hold values from 0.05 to 0.6
- expert_gate: bfloat16 [128, 2048, 512], P('ep'), may hold values from -0.125 to 0.125
- expert_up: bfloat16 [128, 2048, 512], P('ep'), may hold values from -0.125 to 0.125
- expert_down: bfloat16 [128, 512, 2048], P('ep'), may hold values from -0.25 to 0.25
- shared_gate: bfloat16 [2048, 512], replicated, may hold values from -0.125 to 0.125
- shared_up: bfloat16 [2048, 512], replicated, may hold values from -0.125 to 0.125
- shared_down: bfloat16 [512, 2048], replicated, may hold values from -0.25 to 0.25
Outputs:
- layer_out: bfloat16 [8192, 2048], P('ep')
- next_real: float32 [8192, 4096], P('ep')
- next_imag: float32 [8192, 4096], P('ep')
Inputs may be any that keep to these rules, and one draw needn't show every extreme that they name: `routes`: among the rows of one device no expert is named more than 4 times, and in every draw some expert is named exactly 4 times by some device's rows; a token's experts are distinct.
All inputs are finite; a program needn't handle non-finite values.
Results may differ from a plain program's by a relative error of at most 0.0066.
Values may be sent and summed in bfloat16 or wider, within the bound.
No kernel may reach another device: no remote copies, remote signals or barrier semaphores. Data moves between devices by JAX's collectives and lax.ppermute only.
A program may use at most 128 MiB of HBM per device.

v0:
```python
import jax
import jax.numpy as jnp
from jax import lax
from jax.sharding import PartitionSpec as P

norm_eps = 1e-06


def scaled_norm(row_block, norm_gain):
    return (
        row_block
        * lax.rsqrt(jnp.mean(row_block * row_block, axis=-1, keepdims=True) + norm_eps)
        * norm_gain
    )


def state_step(
    branch_in,
    state_real,
    state_imag,
    decay_rate,
    frequency,
    log_step,
    input_real,
    input_imag,
    output_matrix_real,
    output_matrix_imaginary,
    skip_gain,
):
    seq_count = branch_in.shape[0]
    group_count, state_count = decay_rate.shape
    chan_count = input_real.shape[2]
    step_size = jnp.exp(log_step)[:, None]
    magnitude = jnp.exp(-decay_rate * step_size)
    abar_re = magnitude * jnp.cos(frequency * step_size)
    abar_im = magnitude * jnp.sin(frequency * step_size)
    lam_re = -decay_rate
    denominator = lam_re * lam_re + frequency * frequency
    numer_re = abar_re - 1.0
    coef_re = (numer_re * lam_re + abar_im * frequency) / denominator
    coef_im = (abar_im * lam_re - numer_re * frequency) / denominator
    b_real = input_real.astype(jnp.float32)
    b_imag = input_imag.astype(jnp.float32)
    bbar_re = coef_re[..., None] * b_real - coef_im[..., None] * b_imag
    bbar_im = coef_re[..., None] * b_imag + coef_im[..., None] * b_real
    feed_rows = branch_in.astype(jnp.float32).reshape(seq_count, group_count, chan_count)
    forcing_real = jnp.einsum("tgc,gpc->tgp", feed_rows, bbar_re, precision=lax.Precision.HIGHEST)
    drive_im = jnp.einsum("tgc,gpc->tgp", feed_rows, bbar_im, precision=lax.Precision.HIGHEST)
    old_re = state_real.reshape(seq_count, group_count, state_count)
    old_im = state_imag.reshape(seq_count, group_count, state_count)
    fresh_real = abar_re * old_re - abar_im * old_im + forcing_real
    fresh_imaginary = abar_re * old_im + abar_im * old_re + drive_im
    state_readout = jnp.einsum(
        "ukb,krb->ukr",
        fresh_real,
        output_matrix_real.astype(jnp.float32),
        precision=lax.Precision.HIGHEST,
    ) - jnp.einsum(
        "ukb,krb->ukr",
        fresh_imaginary,
        output_matrix_imaginary.astype(jnp.float32),
        precision=lax.Precision.HIGHEST,
    )
    mixed_rows = state_readout.reshape(
        seq_count, group_count * chan_count
    ) + skip_gain * branch_in.astype(jnp.float32)
    activated = jax.nn.gelu(mixed_rows).astype(jnp.bfloat16)
    return (activated, fresh_real.reshape(seq_count, -1), fresh_imaginary.reshape(seq_count, -1))


def expert_rows(row_block, w_gate, w_up, w_down):
    gate_part = jnp.dot(row_block, w_gate, preferred_element_type=jnp.float32)
    up_part = jnp.dot(row_block, w_up, preferred_element_type=jnp.float32)
    hidden = (jax.nn.silu(gate_part) * up_part).astype(jnp.bfloat16)
    return jnp.dot(hidden, w_down, preferred_element_type=jnp.float32)


def mixer_residual(residual, activated, glu_value, glu_gate, mix_gain):
    value_part = jnp.dot(activated, glu_value, preferred_element_type=jnp.float32)
    gate_part = jnp.dot(activated, glu_gate, preferred_element_type=jnp.float32)
    branch = value_part * jax.nn.sigmoid(gate_part)
    return (residual.astype(jnp.float32) + scaled_norm(branch, mix_gain)).astype(jnp.bfloat16)


def serve_rows(
    residual, branch_in, state_real, state_imag, routes, route_weights, params, capacity
):
    (
        decay_rate,
        frequency,
        log_step,
        input_real,
        input_imag,
        output_matrix_real,
        output_matrix_imaginary,
        skip_gain,
        glu_value,
        glu_gate,
        mix_gain,
        moe_in_gain,
        moe_out_gain,
        expert_gate,
        expert_up,
        expert_down,
        shared_gate,
        shared_up,
        shared_down,
    ) = params
    activated, next_real, next_imag = state_step(
        branch_in,
        state_real,
        state_imag,
        decay_rate,
        frequency,
        log_step,
        input_real,
        input_imag,
        output_matrix_real,
        output_matrix_imaginary,
        skip_gain,
    )
    resid_mid = mixer_residual(residual, activated, glu_value, glu_gate, mix_gain)
    normed = scaled_norm(resid_mid.astype(jnp.float32), moe_in_gain).astype(jnp.bfloat16)
    seq_count, hidden_width = normed.shape
    top_count = routes.shape[1]
    expert_count = lax.axis_size("ep")
    flat_routes = routes.reshape(-1)
    assign_count = seq_count * top_count
    position = jnp.arange(assign_count, dtype=jnp.int32)
    earlier = (flat_routes[:, None] == flat_routes[None, :]) & (
        position[None, :] < position[:, None]
    )
    slot_rank = jnp.sum(earlier.astype(jnp.int32), axis=1)
    slot_index = flat_routes * capacity + slot_rank
    slot_source = (
        jnp.full((expert_count * capacity,), seq_count, jnp.int32)
        .at[slot_index]
        .set(position // top_count)
    )
    padded = jnp.concatenate([normed, jnp.zeros((1, hidden_width), jnp.bfloat16)], axis=0)
    outgoing = padded[slot_source].reshape(expert_count, capacity, hidden_width)
    received_rows = lax.all_to_all(outgoing, "ep", split_axis=0, concat_axis=0, tiled=True)
    source_count = received_rows.shape[0]
    item_count = received_rows.shape[1]
    produced = expert_rows(
        received_rows.reshape(-1, hidden_width), expert_gate[0], expert_up[0], expert_down[0]
    ).astype(jnp.bfloat16)
    returned = lax.all_to_all(
        produced.reshape(source_count, item_count, hidden_width),
        "ep",
        split_axis=0,
        concat_axis=0,
        tiled=True,
    )
    per_assign = (
        returned.reshape(-1, hidden_width)[slot_index]
        .reshape(seq_count, top_count, hidden_width)
        .astype(jnp.float32)
    )
    routed = jnp.sum(per_assign * route_weights[..., None], axis=1)
    shared = expert_rows(normed, shared_gate, shared_up, shared_down)
    combined = shared + routed
    layer_out = (resid_mid.astype(jnp.float32) + scaled_norm(combined, moe_out_gain)).astype(
        jnp.bfloat16
    )
    return (layer_out, next_real, next_imag)


def per_device(
    residual,
    branch_in,
    state_real,
    state_imag,
    decay_rate,
    frequency,
    log_step,
    input_real,
    input_imag,
    output_matrix_real,
    output_matrix_imaginary,
    skip_gain,
    glu_value,
    glu_gate,
    mix_gain,
    moe_in_gain,
    moe_out_gain,
    routes,
    route_weights,
    expert_gate,
    expert_up,
    expert_down,
    shared_gate,
    shared_up,
    shared_down,
):
    params = (
        decay_rate,
        frequency,
        log_step,
        input_real,
        input_imag,
        output_matrix_real,
        output_matrix_imaginary,
        skip_gain,
        glu_value,
        glu_gate,
        mix_gain,
        moe_in_gain,
        moe_out_gain,
        expert_gate,
        expert_up,
        expert_down,
        shared_gate,
        shared_up,
        shared_down,
    )
    seq_dev = residual.shape[0]
    capacity = max(2, 4 * seq_dev * routes.shape[1] // (3 * lax.axis_size("ep")))
    return serve_rows(
        residual, branch_in, state_real, state_imag, routes, route_weights, params, capacity
    )


def solution(mesh):
    return jax.shard_map(
        per_device,
        mesh=mesh,
        in_specs=(
            P("ep", None),
            P("ep", None),
            P("ep", None),
            P("ep", None),
            P(),
            P(),
            P(),
            P(),
            P(),
            P(),
            P(),
            P(),
            P(),
            P(),
            P(),
            P(),
            P(),
            P("ep", None),
            P("ep", None),
            P("ep", None, None),
            P("ep", None, None),
            P("ep", None, None),
            P(),
            P(),
            P(),
        ),
        out_specs=(P("ep", None), P("ep", None), P("ep", None)),
        check_vma=False,
    )
```

profile of v0, /device:TPU:1, one launch (start us, length us, event | category | flops | bytes accessed | tf_op | source)
XLA Modules:
  0.0 162.2 jit_solution(14175542040861350788)
XLA Ops:
  0.7 0.8 broadcast_multiply_fusion
  1.5 0.8 copy.56
  2.3 0.7 exp.17
  2.9 1.1 copy.51
  4.0 3.2 %copy.49 = f32[64,4096]{0,1:T(8,128)} copy(f32[64,4096]{1,0:T(8,128)} %param.27) | data formatting | bytes 2097152 | tf_op args[2]
  7.2 3.2 %copy.50 = f32[64,4096]{0,1:T(8,128)} copy(f32[64,4096]{1,0:T(8,128)} %param.28) | data formatting | bytes 2097152 | tf_op args[3]
  10.7 6.0 %bitcast_add_fusion = f32[64,64,64]{0,2,1:T(8,128)} fusion(f32[64,64,64]{0,2,1:T(8,128)} %bitcast.45, f32[64,64,64]{0,2,1:T(8,128)} %bitcast.47, bf16[64,64,16]{0,2,1:T(8,128)(2,1)S(1)} %bitcast.51, f32[64,64]{1,0:T(8,128)S(1)} %get-tuple-element.17, f32[64,64]{1,0:T(8,128)S(1)} %get-tuple-element.15, bf16[64,64,16]{1,2,0:T(8,128)(2,1)S(1)} %copy-done.5, ...), kind=kOutput, calls=%fused_computation.16 | convolution fusion | flops 51707904 | bytes 3604480 | tf_op jit(solution)/shard_map/tgc,gpc->tgp/dot_general | solution.py:48
  16.7 4.1 %bitcast_add_fusion.1 = f32[64,64,64]{0,2,1:T(8,128)} fusion(f32[64,64,64]{0,2,1:T(8,128)S(1)} %bitcast.48, f32[64,64,64]{0,2,1:T(8,128)S(1)} %bitcast.46, bf16[64,64,16]{0,2,1:T(8,128)(2,1)S(1)} %bitcast.52, f32[64,64]{1,0:T(8,128)S(1)} %get-tuple-element.17, f32[64,64]{1,0:T(8,128)S(1)} %get-tuple-element.15, bf16[64,64,16]{1,2,0:T(8,128)(2,1)S(1)} %copy-done.5, ...), kind=kOutput, calls=%fused_computation.17 | convolution fusion | flops 51707904 | bytes 3604480 | tf_op jit(solution)/shard_map/tgc,gpc->tgp/dot_general | solution.py:47
  21.4 2.9 %scatter_custom_fusion = s32[512]{0:T(512)S(1)} fusion(s32[384]{0:T(512)S(1)} %fusion.48, s32[384]{0:T(512)S(1)} %add_select_fusion, s32[]{:T(128)} %constant.14.clone.1), kind=kCustom, calls=%fused_computation.81 | custom fusion | bytes 2052 | tf_op jit(solution)/shard_map/scatter | solution.py:138
  24.3 2.8 %fusion.53 = f32[64,64,16]{1,2,0:T(8,128)S(1)} fusion(f32[64,64,64]{0,2,1:T(8,128)} %bitcast_add_fusion.1, bf16[64,16,64]{2,1,0:T(8,128)(2,1)S(1)} %copy-done.9), kind=kOutput, calls=%fused_computation.88 | convolution fusion | flops 50331648 | bytes 1441792 | tf_op jit(solution)/shard_map/ukb,krb->ukr/dot_general | solution.py:53
  27.2 1.1 convolution_subtract_fusion
  28.7 3.2 %fusion.2 = f32[64,2048]{1,0:T(8,128)S(1)} fusion(bf16[64,1024]{1,0:T(8,128)(2,1)S(1)} %fusion.34, bf16[1024,2048]{1,0:T(8,128)(2,1)} %param.38), kind=kOutput, calls=%fused_computation.10 | convolution fusion | flops 268828672 | bytes 4849664 | tf_op jit(solution)/shard_map/dot_general | solution.py:80
  32.1 1.0 multiply_reduce_fusion.2
  33.1 0.3 fusion.22
  33.6 3.3 %gather_fusion = bf16[512,2048]{1,0:T(8,128)(2,1)} fusion(bf16[65,2048]{1,0:T(8,128)(2,1)S(1)} %concatenate.3, s32[1024]{0:T(1024)S(1)} %pad_clamp_fusion.1), kind=kCustom, calls=%fused_computation | custom fusion | bytes 4196352 | tf_op jit(solution)/shard_map/gather | solution.py:141
  36.9 4.1 %reshape.108 = bf16[128,4,2048]{2,1,0:T(4,128)(2,1)} reshape(bf16[512,2048]{1,0:T(8,128)(2,1)} %gather_fusion) | data formatting | bytes 4194304 | tf_op jit(solution)/shard_map/reshape | solution.py:141
  41.0 42.1 %all_to_all.10 = bf16[128,4,2048]{2,1,0:T(4,128)(2,1)} all-to-all(bf16[128,4,2048]{2,1,0:T(4,128)(2,1)} %reshape.108), channel_id=1, replica_groups=mesh['ep'=128] {'ep'}, dimensions={0} | all-to-all | bytes 4194304 | tf_op jit(solution)/shard_map/all_to_all | solution.py:142
  83.1 4.0 %reshape.109 = bf16[512,2048]{1,0:T(8,128)(2,1)} reshape(bf16[128,4,2048]{2,1,0:T(4,128)(2,1)} %all_to_all.10) | data formatting | bytes 4194304 | tf_op jit(solution)/shard_map/reshape | solution.py:146
  87.0 4.4 %fusion.6 = f32[512,512]{1,0:T(8,128)} fusion(bf16[512,2048]{1,0:T(8,128)(2,1)} %reshape.109, bf16[1,2048,512]{2,1,0:T(8,128)(2,1)} %param.44), kind=kOutput, calls=%fused_computation.14 | convolution fusion | flops 1073741824 | bytes 5242880 | tf_op jit(solution)/shard_map/dot_general | solution.py:72
  91.5 6.3 %convolution_convert_fusion = bf16[512,2048]{1,0:T(8,128)(2,1)} fusion(bf16[1,512,2048]{2,1,0:T(8,128)(2,1)S(1)} %copy-done, bf16[512,2048]{1,0:T(8,128)(2,1)} %reshape.109, bf16[1,2048,512]{2,1,0:T(8,128)(2,1)} %param.45, f32[512,512]{1,0:T(8,128)} %fusion.6), kind=kOutput, calls=%fused_computation.4 | convolution fusion | flops 2150105088 | bytes 9437184 | tf_op jit(solution)/shard_map/dot_general | solution.py:75
  97.7 4.2 %reshape.110 = bf16[128,4,2048]{2,1,0:T(4,128)(2,1)} reshape(bf16[512,2048]{1,0:T(8,128)(2,1)} %convolution_convert_fusion) | data formatting | bytes 4194304 | tf_op jit(solution)/shard_map/reshape | solution.py:149
  101.9 5.6 %all-to-all-start.1 = ((bf16[128,4,2048]{2,1,0:T(4,128)(2,1)}), bf16[128,4,2048]{2,1,0:T(4,128)(2,1)}, u32[]{:S(2)}, u32[]{:S(2)}) async-start(bf16[128,4,2048]{2,1,0:T(4,128)(2,1)} %reshape.110), calls=%async_computation.1 | async-start | bytes 4194304 | tf_op jit(solution)/shard_map/all_to_all | solution.py:148
  107.6 3.1 %copy.59 = f32[64,4096]{1,0:T(8,128)} copy(f32[64,4096]{0,1:T(8,128)} %bitcast.50) | data formatting | bytes 2097152
  110.8 3.1 %copy.58 = f32[64,4096]{1,0:T(8,128)} copy(f32[64,4096]{0,1:T(8,128)} %bitcast.49) | data formatting | bytes 2097152
  113.9 2.1 %fusion.54 = f32[64,512]{1,0:T(8,128)S(1)} fusion(bf16[64,2048]{1,0:T(8,128)(2,1)S(1)} %fusion.24, bf16[2048,512]{1,0:T(8,128)(2,1)} %param.47), kind=kOutput, calls=%fused_computation.89 | convolution fusion | flops 134217728 | bytes 2490368 | tf_op jit(solution)/shard_map/dot_general | solution.py:72
  116.0 21.8 %all-to-all-done.1 = bf16[128,4,2048]{2,1,0:T(4,128)(2,1)} async-done(((bf16[128,4,2048]{2,1,0:T(4,128)(2,1)}), bf16[128,4,2048]{2,1,0:T(4,128)(2,1)}, u32[]{:S(2)}, u32[]{:S(2)}) %all-to-all-start.1) | async-done | bytes 2097184 | tf_op jit(solution)/shard_map/all_to_all | solution.py:148
  137.7 3.9 %reshape.111 = bf16[512,2048]{1,0:T(8,128)(2,1)} reshape(bf16[128,4,2048]{2,1,0:T(4,128)(2,1)} %all-to-all-done.1) | data formatting | bytes 4194304 | tf_op jit(solution)/shard_map/reshape | solution.py:156
  141.7 6.9 %gather_fusion.1 = bf16[384,2048]{1,0:T(8,128)(2,1)} fusion(bf16[512,2048]{1,0:T(8,128)(2,1)} %reshape.111, s32[1024]{0:T(1024)S(1)} %pad_clamp_fusion), kind=kCustom, calls=%fused_computation.1 | custom fusion | bytes 3147264 | tf_op jit(solution)/shard_map/gather | solution.py:156
  148.6 3.9 %reshape.114 = f32[64,6,2048]{2,1,0:T(8,128)} reshape(bf16[384,2048]{1,0:T(8,128)(2,1)} %gather_fusion.1) | data formatting | bytes 4718592 | tf_op jit(solution)/shard_map/convert_element_type | solution.py:158
  152.5 3.7 %multiply_reduce_fusion = f32[64,2048]{1,0:T(8,128)S(1)} fusion(f32[64,6,2048]{2,1,0:T(8,128)} %reshape.114, f32[64,6]{1,0:T(8,128)S(1)} %copy.57), kind=kLoop, calls=%fused_computation.3 | loop fusion | flops 1441792 | bytes 3671552 | tf_op jit(solution)/shard_map/reduce_sum | solution.py:160
  156.3 4.0 %multiply_reduce_fusion.1 = (f32[64]{0:T(128)S(1)}, f32[64,2048]{1,0:T(8,128)}) fusion(f32[64,2048]{1,0:T(8,128)S(1)} %multiply_reduce_fusion, bf16[512,2048]{1,0:T(8,128)(2,1)} %param.49, bf16[64,2048]{1,0:T(8,128)(2,1)S(1)} %fusion.24, bf16[2048,512]{1,0:T(8,128)(2,1)} %param.48, f32[64,512]{1,0:T(8,128)S(1)} %fusion.54), kind=kOutput, calls=%fused_computation.39 | convolution fusion | flops 269025216 | bytes 5636352 | tf_op jit(solution)/shard_map/dot_general | solution.py:75
  160.3 1.9 %fusion.25 = bf16[64,2048]{1,0:T(8,128)(2,1)} fusion(bf16[64,2048]{1,0:T(8,128)(2,1)S(1)} %get-tuple-element.13, f32[64,2048]{1,0:T(8,128)} %get-tuple-element.21, f32[2048]{0:T(1024)S(1)} %copy-done.15, f32[64]{0:T(128)S(1)} %add_rsqrt_fusion), kind=kLoop, calls=%fused_computation.38 | loop fusion | flops 655360 | bytes 1057024 | tf_op jit(solution)/shard_map/convert_element_type | solution.py:163
  (54 shorter events, 1.7 us)
Async XLA Ops:
  0.6 90.8 %copy-start = (bf16[1,512,2048]{2,1,0:T(8,128)(2,1)S(1)}, bf16[1,512,2048]{2,1,0:T(8,128)(2,1)}, u32[]{:S(2)}) copy-start(bf16[1,512,2048]{2,1,0:T(8,128)(2,1)} %param.46) | copy-start | bytes 6291460
  7.2 3.2 %copy-start.11 = (f32[64,64]{1,0:T(8,128)S(1)}, f32[64,64]{1,0:T(8,128)}, u32[]{:S(2)}) copy-start(f32[64,64]{1,0:T(8,128)} %param.30) | copy-start | bytes 49156
  7.2 3.2 %copy-start.12 = (f32[64,64]{1,0:T(8,128)S(1)}, f32[64,64]{1,0:T(8,128)}, u32[]{:S(2)}) copy-start(f32[64,64]{1,0:T(8,128)} %param.29) | copy-start | bytes 49156
  7.2 3.4 %copy-start.5 = (bf16[64,64,16]{1,2,0:T(8,128)(2,1)S(1)}, bf16[64,64,16]{1,2,0:T(8,128)(2,1)}, u32[]{:S(2)}) copy-start(bf16[64,64,16]{1,2,0:T(8,128)(2,1)} %param.32) | copy-start | bytes 393220
  7.2 3.4 %copy-start.6 = (bf16[64,64,16]{1,2,0:T(8,128)(2,1)S(1)}, bf16[64,64,16]{1,2,0:T(8,128)(2,1)}, u32[]{:S(2)}) copy-start(bf16[64,64,16]{1,2,0:T(8,128)(2,1)} %param.33) | copy-start | bytes 393220
  10.6 6.0 %copy-start.1 = (f32[64,4096]{0,1:T(8,128)S(1)}, f32[64,4096]{0,1:T(8,128)}, u32[]{:S(2)}) copy-start(f32[64,4096]{0,1:T(8,128)} %copy.49) | copy-start | bytes 3145732
  10.6 6.0 %copy-start.2 = (f32[64,4096]{0,1:T(8,128)S(1)}, f32[64,4096]{0,1:T(8,128)}, u32[]{:S(2)}) copy-start(f32[64,4096]{0,1:T(8,128)} %copy.50) | copy-start | bytes 3145732
  16.7 7.7 %copy-start.9 = (bf16[64,16,64]{2,1,0:T(8,128)(2,1)S(1)}, bf16[64,16,64]{2,1,0:T(8,128)(2,1)}, u32[]{:S(2)}) copy-start(bf16[64,16,64]{2,1,0:T(8,128)(2,1)} %param.34) | copy-start | bytes 393220
  20.7 6.5 %copy-start.10 = (bf16[64,16,64]{2,1,0:T(8,128)(2,1)S(1)}, bf16[64,16,64]{2,1,0:T(8,128)(2,1)}, u32[]{:S(2)}) copy-start(bf16[64,16,64]{2,1,0:T(8,128)(2,1)} %param.35) | copy-start | bytes 393220
  24.3 2.9 %copy-start.3 = (f32[64,64,64]{0,2,1:T(8,128)S(1)}, f32[64,64,64]{0,2,1:T(8,128)}, u32[]{:S(2)}) copy-start(f32[64,64,64]{0,2,1:T(8,128)} %bitcast_add_fusion) | copy-start | bytes 3145732
  27.2 1.3 copy-start.7
  27.2 1.3 copy-start.16
  28.7 3.5 %copy-start.4 = (bf16[1024,2048]{1,0:T(8,128)(2,1)S(1)}, bf16[1024,2048]{1,0:T(8,128)(2,1)}, u32[]{:S(2)}) copy-start(bf16[1024,2048]{1,0:T(8,128)(2,1)} %param.37) | copy-start | bytes 12582916
  32.1 1.0 copy-start.8
  32.1 1.0 copy-start.13
  32.1 1.3 copy-start.14
  101.9 5.6 %copy-start.17 = (f32[64,6]{0,1:T(8,128)S(1)}, f32[64,6]{0,1:T(8,128)}, u32[]{:S(2)}) copy-start(f32[64,6]{0,1:T(8,128)} %param.43) | copy-start | bytes 4612
  101.9 35.8 %all-to-all-start.1 = ((bf16[128,4,2048]{2,1,0:T(4,128)(2,1)}), bf16[128,4,2048]{2,1,0:T(4,128)(2,1)}, u32[]{:S(2)}, u32[]{:S(2)}) async-start(bf16[128,4,2048]{2,1,0:T(4,128)(2,1)} %reshape.110), calls=%async_computation.1 | async-start | bytes 4194304 | tf_op jit(solution)/shard_map/all_to_all | solution.py:148
  156.3 4.1 %copy-start.15 = (f32[2048]{0:T(1024)S(1)}, f32[2048]{0:T(1024)}, u32[]{:S(2)}) copy-start(f32[2048]{0:T(1024)} %param.41) | copy-start | bytes 24580
where the time goes:
time: 163 us; the launch traced here: 162 us
  local copies, waits for them, and re-layouts  49.4 us (30%)
  blocking collectives  42.1 us (26%)
  matrix products  35 us (21%)
  waiting for transfers between devices  21.8 us (13%)
  other arithmetic  7.54 us (5%)
  starting transfers between devices  5.59 us (3%)
    all_to_all x1, blocking collectives, serve_rows(): lax.all_to_all(outgoing, 'ep', split_axis=0, concat_axis=0, tiled=True)  42.1 us
    all_to_all x1, waiting for transfers between devices, serve_rows(): lax.all_to_all(produced.reshape(source_count, item_count, hidden_width),...  21.8 us
    unnamed x43, local copies, waits for them, and re-layouts  14.9 us
    dot_general x2, matrix products, expert_rows(): return jnp.dot(hidden, w_down, preferred_element_type=jnp.float32)  10.3 us
    gather x1, local copies, waits for them, and re-layouts, serve_rows(): returned.reshape(-1, hidden_width)[slot_index]  6.93 us
    dot_general x2, matrix products, expert_rows(): gate_part = jnp.dot(row_block, w_gate, preferred_element_type=jnp.float32)  6.5 us
    dot_general x1, matrix products, state_step(): jnp.einsum('tgc,gpc->tgp', feed_rows, bbar_im, precision=lax.Precision.HI...  5.99 us
    all_to_all x1, starting transfers between devices, serve_rows(): lax.all_to_all(produced.reshape(source_count, item_count, hidden_width),...  5.59 us
  transfers between devices with their start and end apart: 1, of which 1 were waited for; matrix products, arithmetic and copies ran while one was open for 5% of the time, Pallas kernels for 0%

commit v1 on v0

v1 whole, which is shorter than its diff:
```python
import functools

import jax
import jax.numpy as jnp
from jax import lax
from jax.experimental import pallas as pl
from jax.experimental.pallas import tpu as pltpu
from jax.sharding import PartitionSpec as P

norm_eps = 1e-06
f32 = jnp.float32
bf16 = jnp.bfloat16

CHUNK = 256
CAPACITY = 4
PARTS = 4


def iota(shape, dim):
    return lax.broadcasted_iota(jnp.int32, shape, dim)


def dot(a, b):
    return jnp.dot(a, b, preferred_element_type=f32)


def sin_cos(x):
    turns = jnp.floor(x * 0.6366197723675814 + 0.5)
    r = ((x - turns * 1.5703125) - turns * 4.837512969970703125e-4) - turns * 7.54978995489188216e-8
    z = r * r
    s = r + r * z * ((-1.9515295891e-4 * z + 8.3321608736e-3) * z - 1.6666654611e-1)
    c = 1.0 - 0.5 * z + z * z * (
        (2.443315711809948e-5 * z - 1.388731625493765e-3) * z + 4.166664568298827e-2
    )
    quarter = turns.astype(jnp.int32) & 3
    odd = (quarter & 1) == 1
    sin_x = jnp.where(odd, c, s)
    cos_x = jnp.where(odd, s, c)
    sin_x = jnp.where(quarter >= 2, -sin_x, sin_x)
    cos_x = jnp.where((quarter == 1) | (quarter == 2), -cos_x, cos_x)
    return sin_x, cos_x


def split(x):
    hi = x.astype(bf16)
    return hi, (x - hi.astype(f32)).astype(bf16)


def route_code(routes):
    top, seq = routes.shape
    experts = 128
    row = iota((experts, seq), 0)
    named = jnp.zeros((experts, seq), f32)
    for k in range(top):
        named = named + jnp.where(row == routes[k : k + 1, :], 1.0, 0.0)
    before = jnp.where(iota((seq, seq), 0) < iota((seq, seq), 1), 1.0, 0.0).astype(bf16)
    rank = dot(named.astype(bf16), before)
    return jnp.where(named > 0.5, rank, -1.0)


def spread_rows(block):
    one_hot = jnp.where(iota((CHUNK, 16), 0) // 16 == iota((CHUNK, 16), 1), 1.0, 0.0)
    return dot(one_hot.astype(bf16), block.astype(bf16))


def slot_pattern(seq):
    i = iota((CHUNK, PARTS * seq), 0)
    j = iota((CHUNK, PARTS * seq), 1)
    return jnp.where((i // 4) % 4 == j // seq, (i % 4).astype(f32), -2.0)


def rms_scale(x):
    return lax.rsqrt(jnp.mean(x * x, axis=-1, keepdims=True) + norm_eps)


def mixer_kernel(
    u_ref, sr_ref, si_ref, decay_ref, freq_ref, log_ref, inr_ref, ini_ref, cr_ref, ci_ref,
    skip_ref, gv_ref, gg_ref, res_ref, mix_ref, gain_ref, routes_ref,
    nr_ref, ni_ref, mid_ref, normed_ref, out_ref,
    br, bi, cr, ci, acc_v, acc_g,
):
    step = pl.program_id(0)
    groups, states = decay_ref.shape
    chans = inr_ref.shape[0] // groups
    seq = u_ref.shape[0]
    wide = groups * states

    @pl.when(step == 0)
    def _():
        for ref in (br, bi, cr, ci):
            ref[...] = jnp.zeros_like(ref)
        acc_v[...] = jnp.zeros_like(acc_v)
        acc_g[...] = jnp.zeros_like(acc_g)

    logs = log_ref[...]
    pick = iota((groups, logs.shape[1]), 1) == iota((groups, logs.shape[1]), 0) + step * groups
    step_size = jnp.exp(jnp.sum(jnp.where(pick, logs, 0.0), axis=1, keepdims=True))
    decay = decay_ref[...]
    freq = freq_ref[...]
    magnitude = jnp.exp(-decay * step_size)
    sin_x, cos_x = sin_cos(freq * step_size)
    a_re = magnitude * cos_x
    a_im = magnitude * sin_x
    lam = -decay
    den = lam * lam + freq * freq
    num = a_re - 1.0
    k_re = (num * lam + a_im * freq) / den
    k_im = (a_im * lam - num * freq) / den

    lane_group = iota((groups, wide), 1) // states
    own = iota((groups, wide), 0) == lane_group

    def flat(x):
        twice = jnp.concatenate([x, x], axis=1)
        tiled = jnp.concatenate([twice] * (groups // 2), axis=1)
        return jnp.sum(jnp.where(own, tiled, 0.0), axis=0, keepdims=True)

    a_re, a_im, k_re, k_im = flat(a_re), flat(a_im), flat(k_re), flat(k_im)

    rows = groups * chans
    patch = (iota((rows, 2 * states), 0) // chans) % 2 == iota((rows, 2 * states), 1) // states
    for ref, src in ((br, inr_ref), (bi, ini_ref), (cr, cr_ref), (ci, ci_ref)):
        x = src[...].astype(f32)
        x = jnp.where(patch, jnp.concatenate([x, x], axis=1), 0.0).astype(bf16)
        for j in range(groups // 2):
            r = slice(2 * chans * j, 2 * chans * (j + 1))
            ref[r, 2 * states * j : 2 * states * (j + 1)] = x[r]

    u = u_ref[...]
    f_re = dot(u, br[...])
    f_im = dot(u, bi[...])
    old_re = sr_ref[...]
    old_im = si_ref[...]
    new_re = a_re * old_re - a_im * old_im + (k_re * f_re - k_im * f_im)
    new_im = a_re * old_im + a_im * old_re + (k_re * f_im + k_im * f_re)
    nr_ref[...] = new_re
    ni_ref[...] = new_im

    def read(x, m):
        hi, lo = split(x)
        both = lax.dot_general(
            jnp.concatenate([hi, lo], axis=0), m, (((1,), (1,)), ((), ())),
            preferred_element_type=f32,
        )
        return both[:seq] + both[seq:]

    mixed = read(new_re, cr[...]) - read(new_im, ci[...]) + skip_ref[...] * u.astype(f32)
    act = jax.nn.gelu(mixed).astype(bf16)
    acc_v[...] += dot(act, gv_ref[...])
    acc_g[...] += dot(act, gg_ref[...])

    @pl.when(step == pl.num_programs(0) - 1)
    def _():
        branch = acc_v[...] * jax.nn.sigmoid(acc_g[...])
        mid = (res_ref[...].astype(f32) + branch * rms_scale(branch) * mix_ref[...]).astype(bf16)
        mid_ref[...] = mid
        mid = mid.astype(f32)
        normed = (mid * rms_scale(mid) * gain_ref[...]).astype(bf16)
        normed_ref[...] = normed
        part = normed.shape[1] // PARTS
        stacked = jnp.concatenate(
            [normed[:, part * q : part * (q + 1)] for q in range(PARTS)], axis=0
        )
        code = route_code(routes_ref[...])
        code = jnp.concatenate([code] * PARTS, axis=1)
        want = slot_pattern(seq)
        for c in range(out_ref.shape[0] // CHUNK):
            here = spread_rows(code[16 * c : 16 * (c + 1)])
            select = jnp.where(here == want, 1.0, 0.0).astype(bf16)
            out_ref[CHUNK * c : CHUNK * (c + 1), :] = dot(select, stacked).astype(bf16)


def run_mixer(
    u, sr, si, decay, freq, log_step, inr, ini, cr, ci, skip, gv, gg, res, mix, gain, routes
):
    seq, width = u.shape
    model = res.shape[1]
    steps = 4
    groups, states = decay.shape
    part = model // PARTS
    gb, cb, wb = groups // steps, width // steps, groups * states // steps
    cols = lambda n: pl.BlockSpec((seq, n), lambda i: (0, i))
    rows = lambda r, n: pl.BlockSpec((r, n), lambda i: (i, 0))
    whole = lambda x: pl.BlockSpec(x.shape, lambda i: (0, 0))
    out_rows = 128 * CAPACITY * PARTS
    return pl.pallas_call(
        mixer_kernel,
        grid=(steps,),
        in_specs=[
            cols(cb), cols(wb), cols(wb), rows(gb, states), rows(gb, states), whole(log_step),
            rows(cb, states), rows(cb, states), rows(cb, states), rows(cb, states),
            pl.BlockSpec((1, cb), lambda i: (0, i)),
            rows(cb, model), rows(cb, model), whole(res), whole(mix), whole(gain), whole(routes),
        ],
        out_specs=[
            cols(wb), cols(wb),
            pl.BlockSpec((seq, model), lambda i: (0, 0)),
            pl.BlockSpec((seq, model), lambda i: (0, 0)),
            pl.BlockSpec((out_rows, part), lambda i: (0, 0)),
        ],
        out_shape=[
            jax.ShapeDtypeStruct(sr.shape, f32),
            jax.ShapeDtypeStruct(si.shape, f32),
            jax.ShapeDtypeStruct((seq, model), bf16),
            jax.ShapeDtypeStruct((seq, model), bf16),
            jax.ShapeDtypeStruct((out_rows, part), bf16),
        ],
        scratch_shapes=[pltpu.VMEM((cb, wb), bf16)] * 4 + [pltpu.VMEM((seq, model), f32)] * 2,
        name="mixer",
    )(u, sr, si, decay, freq, log_step, inr, ini, cr, ci, skip, gv, gg, res, mix, gain, routes)


def swap_matrix(back):
    i = iota((CHUNK, CHUNK), 1 if back else 0)
    j = iota((CHUNK, CHUNK), 0 if back else 1)
    source = ((i // 4) % 16) * 16 + (i // 64) * 4 + i % 4
    return jnp.where(source == j, 1.0, 0.0).astype(bf16)


def expert_kernel(y_ref, wg_ref, wu_ref, wd_ref, z_ref):
    model = wg_ref.shape[0]
    part = model // PARTS
    take = CHUNK // PARTS
    order = swap_matrix(False)
    pieces = []
    for c in range(y_ref.shape[0] // CHUNK):
        x = dot(order, y_ref[CHUNK * c : CHUNK * (c + 1), :]).astype(bf16)
        pieces.append(
            jnp.concatenate([x[take * q : take * (q + 1)] for q in range(PARTS)], axis=1)
        )
    x = jnp.concatenate(pieces, axis=0)
    gate = dot(x, wg_ref[...])
    up = dot(x, wu_ref[...])
    hidden = (gate * jax.nn.sigmoid(gate) * up).astype(bf16)
    out = dot(hidden, wd_ref[...]).astype(bf16)
    back = swap_matrix(True)
    for c in range(y_ref.shape[0] // CHUNK):
        o = out[take * c : take * (c + 1)]
        o = jnp.concatenate([o[:, part * q : part * (q + 1)] for q in range(PARTS)], axis=0)
        z_ref[CHUNK * c : CHUNK * (c + 1), :] = dot(back, o).astype(bf16)


def run_expert(y, wg, wu, wd):
    steps = 4
    whole = lambda x: pl.BlockSpec(x.shape, lambda i: (0, 0))
    block = pl.BlockSpec((y.shape[0] // steps, y.shape[1]), lambda i: (i, 0))
    return pl.pallas_call(
        expert_kernel,
        grid=(steps,),
        in_specs=[block, whole(wg), whole(wu), whole(wd)],
        out_specs=block,
        out_shape=jax.ShapeDtypeStruct(y.shape, bf16),
        name="expert",
    )(y, wg, wu, wd)


def shared_kernel(normed_ref, wg_ref, wu_ref, wd_ref, routes_ref, weights_ref, out_ref, mix_ref):
    x = normed_ref[...]
    gate = dot(x, wg_ref[...])
    up = dot(x, wu_ref[...])
    hidden = (gate * jax.nn.sigmoid(gate) * up).astype(bf16)
    out_ref[...] = dot(hidden, wd_ref[...])

    routes = routes_ref[...]
    weights = weights_ref[...]
    top, seq = routes.shape
    code = route_code(routes)
    row = iota(code.shape, 0)
    weight = jnp.zeros(code.shape, f32)
    for k in range(top):
        weight = weight + jnp.where(row == routes[k : k + 1, :], weights[k : k + 1, :], 0.0)
    code = jnp.concatenate([code] * PARTS, axis=1)
    weight = jnp.concatenate([weight] * PARTS, axis=1)
    hi, lo = split(weight)
    want = slot_pattern(seq)
    for c in range(mix_ref.shape[0] // CHUNK):
        r = slice(16 * c, 16 * (c + 1))
        hit = spread_rows(code[r]) == want
        for h, w in enumerate((hi, lo)):
            mix_ref[CHUNK * c : CHUNK * (c + 1), PARTS * seq * h : PARTS * seq * (h + 1)] = (
                jnp.where(hit, spread_rows(w[r]), 0.0).astype(bf16)
            )


def run_shared(normed, wg, wu, wd, routes, weights):
    seq, model = normed.shape
    return pl.pallas_call(
        shared_kernel,
        out_shape=[
            jax.ShapeDtypeStruct((seq, model), f32),
            jax.ShapeDtypeStruct((128 * CAPACITY * PARTS, 2 * PARTS * seq), bf16),
        ],
        cost_estimate=pl.CostEstimate(
            flops=2 * seq * model * wg.shape[1] * 60, bytes_accessed=8 << 20, transcendentals=0
        ),
        name="shared",
    )(normed, wg, wu, wd, routes, weights)


def combine_kernel(z_ref, mix_ref, shared_ref, mid_ref, gain_ref, out_ref):
    seq = mid_ref.shape[0]
    both = lax.dot_general(
        mix_ref[...], z_ref[...], (((0,), (0,)), ((), ())), preferred_element_type=f32
    )
    both = both[: PARTS * seq] + both[PARTS * seq :]
    routed = jnp.concatenate([both[seq * q : seq * (q + 1)] for q in range(PARTS)], axis=1)
    combined = shared_ref[...] + routed
    out_ref[...] = (
        mid_ref[...].astype(f32) + combined * rms_scale(combined) * gain_ref[...]
    ).astype(bf16)


def run_combine(z, mix, shared, mid, gain):
    return pl.pallas_call(
        combine_kernel,
        out_shape=jax.ShapeDtypeStruct(mid.shape, bf16),
        name="combine",
    )(z, mix, shared, mid, gain)


def per_device(
    residual, branch_in, state_real, state_imag, decay_rate, frequency, log_step, input_real,
    input_imag, output_matrix_real, output_matrix_imaginary, skip_gain, glu_value, glu_gate,
    mix_gain, moe_in_gain, moe_out_gain, routes, route_weights, expert_gate, expert_up,
    expert_down, shared_gate, shared_up, shared_down,
):
    states = decay_rate.shape[1]
    model = residual.shape[1]
    part = model // PARTS
    row = lambda v: v.reshape(1, -1)
    inr = jnp.transpose(input_real, (0, 2, 1)).reshape(-1, states)
    ini = jnp.transpose(input_imag, (0, 2, 1)).reshape(-1, states)
    cr = output_matrix_real.reshape(-1, states)
    ci = output_matrix_imaginary.reshape(-1, states)
    routes_t = routes.T
    weights_t = route_weights.T
    next_real, next_imag, mid, normed, outgoing = run_mixer(
        branch_in, state_real, state_imag, decay_rate, frequency, row(log_step), inr, ini, cr, ci,
        row(skip_gain), glu_value, glu_gate, residual, row(mix_gain), row(moe_in_gain), routes_t,
    )

    def exchange(x):
        x = x.reshape(128, PARTS * CAPACITY, part)
        return lax.all_to_all(x, "ep", split_axis=0, concat_axis=0, tiled=True).reshape(-1, part)

    arrived = exchange(outgoing)
    shared, mix = run_shared(normed, shared_gate, shared_up, shared_down, routes_t, weights_t)
    returned = exchange(run_expert(arrived, expert_gate[0], expert_up[0], expert_down[0]))
    layer_out = run_combine(returned, mix, shared, mid, row(moe_out_gain))
    return layer_out, next_real, next_imag


def solution(mesh):
    rows2 = P("ep", None)
    rows3 = P("ep", None, None)
    return jax.shard_map(
        per_device,
        mesh=mesh,
        in_specs=(rows2,) * 4 + (P(),) * 13 + (rows2,) * 2 + (rows3,) * 3 + (P(),) * 3,
        out_specs=(rows2, rows2, rows2),
        check_vma=False,
    )
```

time: 163 us -> 106 us (0.65)
  local copies, waits for them, and re-layouts: 49.4 us -> 1.31 us
  matrix products: 35 us -> 0 us
  Pallas kernels: 0 us -> 33.6 us
  other arithmetic: 7.54 us -> 0 us
  waiting for transfers between devices: 21.8 us -> 24 us
    dot_general x10 -> x0, matrix products: 35 us -> none  [the longest x2 10.3 us: expert_rows(): return jnp.dot(hidden, w_down, preferred_element_type=jnp.float32)]
    pallas_call x0 -> x4, Pallas kernels: none -> 33.6 us  [the longest x1 12.3 us: run_mixer(): pl.pallas_call(mixer_kernel, grid=(steps,), in_specs=[cols(cb), cols(wb),...]
    reshape x5 -> x0, local copies, waits for them, and re-layouts: 16.4 us -> none  [the longest x1 4.15 us: serve_rows(): produced.reshape(source_count, item_count, hidden_width)]
    unnamed x43 -> x2, local copies, waits for them, and re-layouts: 14.9 us -> 1.31 us
    gather x2 -> x0, local copies, waits for them, and re-layouts: 10.2 us -> none  [the longest x1 6.93 us: serve_rows(): returned.reshape(-1, hidden_width)[slot_index]]
    reduce_sum x3 -> x0, other arithmetic: 4.26 us -> none  [the longest x1 3.74 us: serve_rows(): routed = jnp.sum(per_assign * route_weights[..., None], axis=1)]
    convert_element_type x1 -> x0, local copies, waits for them, and re-layouts: 3.89 us -> none  [serve_rows(): per_assign = returned.reshape(-1, hidden_width)[slot_index].reshape(seq_c...]
    scatter x1 -> x0, local copies, waits for them, and re-layouts: 2.91 us -> none  [serve_rows(): slot_source = jnp.full((expert_count * capacity,), seq_count, jnp.int32)....]
  transfers between devices with their start and end apart: 1 -> 1, of which waited for: 1 -> 1; matrix products, arithmetic and copies ran while one was open for 5% -> 0% of each run, Pallas kernels for 0% -> 6%
where the time goes in v1:
time: 106 us
  blocking collectives  42.1 us (40%)
  Pallas kernels  33.6 us (32%)
  waiting for transfers between devices  24 us (23%)
  starting transfers between devices  4.4 us (4%)
  local copies, waits for them, and re-layouts  1.31 us (1%)
    all_to_all x1, blocking collectives, exchange(): lax.all_to_all(x, 'ep', split_axis=0, concat_axis=0, tiled=True)  42.1 us
    all_to_all x1, waiting for transfers between devices, exchange(): lax.all_to_all(x, 'ep', split_axis=0, concat_axis=0, tiled=True)  24 us
    pallas_call x1, Pallas kernels, run_mixer(): pl.pallas_call(mixer_kernel, grid=(steps,), in_specs=[cols(cb), cols(wb),...  12.3 us
    pallas_call x1, Pallas kernels, run_expert(): pl.pallas_call(expert_kernel, grid=(steps,), in_specs=[block, whole(wg),...  10.1 us
    pallas_call x1, Pallas kernels, run_shared(): pl.pallas_call(shared_kernel, out_shape=[jax.ShapeDtypeStruct((seq, model...  6.59 us
    pallas_call x1, Pallas kernels, run_combine(): pl.pallas_call(combine_kernel, out_shape=jax.ShapeDtypeStruct(mid.shape,...  4.52 us
    all_to_all x1, starting transfers between devices, exchange(): lax.all_to_all(x, 'ep', split_axis=0, concat_axis=0, tiled=True)  4.4 us
  transfers between devices with their start and end apart: 1, of which 1 were waited for; matrix products, arithmetic and copies ran while one was open for 0% of the time, Pallas kernels for 6%

profile of v1, /device:TPU:1, one launch (start us, length us, event | category | flops | bytes accessed | tf_op | source)
XLA Modules:
  0.0 106.0 jit_solution(7279907479430765183)
XLA Ops:
  0.6 12.3 %mixer.1 = (f32[64,4096]{1,0:T(8,128)}, f32[64,4096]{1,0:T(8,128)}, bf16[64,2048]{1,0:T(8,128)(2,1)}, bf16[64,2048]{1,0:T(8,128)(2,1)}, bf16[2048,512]{1,0:T(8,128)(2,1)}) custom-call(bf16[64,1024]{1,0:T(8,128)(2,1)} %u_ref.1, f32[64,4096]{1,0:T(8,128)} %sr_ref.1, f32[64,4096]{1,0:T(8,128)} %si_ref.1, f32[64,64]{1,0:T(8,128)} %decay_ref.1, ...), custom_call_target="tpu_custom_call" | custom-call | tf_op jit(solution)/shard_map/mixer/pallas_call | solution.py:186
  12.9 42.1 %all_to_all.10 = bf16[128,16,512]{2,1,0:T(8,128)(2,1)} all-to-all(bf16[128,16,512]{2,1,0:T(8,128)(2,1)} %bitcast.28), channel_id=1, replica_groups=mesh['ep'=128] {'ep'}, dimensions={0} | all-to-all | bytes 4194304 | tf_op jit(solution)/shard_map/all_to_all | solution.py:344
  55.0 10.1 %expert.1 = bf16[2048,512]{1,0:T(8,128)(2,1)} custom-call(bf16[2048,512]{1,0:T(8,128)(2,1)} %bitcast.24, bf16[2048,512]{1,0:T(8,128)(2,1)} %bitcast.25, bf16[2048,512]{1,0:T(8,128)(2,1)} %bitcast.26, bf16[512,2048]{1,0:T(8,128)(2,1)} %bitcast.27), custom_call_target="tpu_custom_call" | custom-call | tf_op jit(solution)/shard_map/expert/pallas_call | solution.py:247
  65.2 4.4 %all-to-all-start.1 = ((bf16[128,16,512]{2,1,0:T(8,128)(2,1)}), bf16[128,16,512]{2,1,0:T(8,128)(2,1)S(1)}, u32[]{:S(2)}, u32[]{:S(2)}) async-start(bf16[128,16,512]{2,1,0:T(8,128)(2,1)} %bitcast.23), calls=%async_computation.1 | async-start | bytes 4194304 | tf_op jit(solution)/shard_map/all_to_all | solution.py:344
  69.6 6.6 %shared.1 = (f32[64,2048]{1,0:T(8,128)}, bf16[2048,512]{1,0:T(8,128)(2,1)}) custom-call(bf16[64,2048]{1,0:T(8,128)(2,1)} %get-tuple-element.11.normed_ref, bf16[2048,512]{1,0:T(8,128)(2,1)} %wg_ref.1, bf16[2048,512]{1,0:T(8,128)(2,1)} %wu_ref.1, bf16[512,2048]{1,0:T(8,128)(2,1)} %wd_ref.1, s32[6,64]{1,0:T(8,128)} %bitcast.38, f32[6,64]{1,0:T(8,128)} %bitcast.40), custom_call_target="tpu_custom_call" | custom-call | flops 8053063680 | bytes 8388608 | tf_op jit(solution)/shard_map/shared/pallas_call | solution.py:287
  76.2 24.0 %all-to-all-done.1 = bf16[128,16,512]{2,1,0:T(8,128)(2,1)S(1)} async-done(((bf16[128,16,512]{2,1,0:T(8,128)(2,1)}), bf16[128,16,512]{2,1,0:T(8,128)(2,1)S(1)}, u32[]{:S(2)}, u32[]{:S(2)}) %all-to-all-start.1) | async-done | bytes 2097184 | tf_op jit(solution)/shard_map/all_to_all | solution.py:344
  100.2 0.0 copy-start
  100.2 1.3 %copy-done = bf16[128,16,512]{2,1,0:T(8,128)(2,1)} copy-done((bf16[128,16,512]{2,1,0:T(8,128)(2,1)}, bf16[128,16,512]{2,1,0:T(8,128)(2,1)S(1)}, u32[]{:S(2)}) %copy-start) | copy-done | bytes 2097176
  101.5 4.5 %combine.1 = bf16[64,2048]{1,0:T(8,128)(2,1)} custom-call(bf16[2048,512]{1,0:T(8,128)(2,1)} %bitcast.22, bf16[2048,512]{1,0:T(8,128)(2,1)} %get-tuple-element.12.mix_ref, f32[64,2048]{1,0:T(8,128)} %get-tuple-element.13.shared_ref, bf16[64,2048]{1,0:T(8,128)(2,1)} %get-tuple-element.14.mid_ref, f32[1,2048]{1,0:T(1,128)} %bitcast.33), custom_call_target="tpu_custom_call" | custom-call | tf_op jit(solution)/shard_map/combine/pallas_call | solution.py:314
Async XLA Ops:
  65.2 35.0 %all-to-all-start.1 = ((bf16[128,16,512]{2,1,0:T(8,128)(2,1)}), bf16[128,16,512]{2,1,0:T(8,128)(2,1)S(1)}, u32[]{:S(2)}, u32[]{:S(2)}) async-start(bf16[128,16,512]{2,1,0:T(8,128)(2,1)} %bitcast.23), calls=%async_computation.1 | async-start | bytes 4194304 | tf_op jit(solution)/shard_map/all_to_all | solution.py:344
  100.2 1.3 %copy-start = (bf16[128,16,512]{2,1,0:T(8,128)(2,1)}, bf16[128,16,512]{2,1,0:T(8,128)(2,1)S(1)}, u32[]{:S(2)}) copy-start(bf16[128,16,512]{2,1,0:T(8,128)(2,1)S(1)} %all-to-all-done.1) | copy-start | bytes 6291460

commit v2 on v1

--- a/solution.py
+++ b/solution.py
@@ -168,6 +168,14 @@
             here = spread_rows(code[16 * c : 16 * (c + 1)])
             select = jnp.where(here == want, 1.0, 0.0).astype(bf16)
             out_ref[CHUNK * c : CHUNK * (c + 1), :] = dot(select, stacked).astype(bf16)
+
+
+def in_hbm(x):
+    return pltpu.with_memory_space_constraint(x, pltpu.HBM)
+
+
+def in_vmem():
+    return pl.BlockSpec(memory_space=pltpu.VMEM)
 
 
 def run_mixer(
@@ -194,9 +202,7 @@
         ],
         out_specs=[
             cols(wb), cols(wb),
-            pl.BlockSpec((seq, model), lambda i: (0, 0)),
-            pl.BlockSpec((seq, model), lambda i: (0, 0)),
-            pl.BlockSpec((out_rows, part), lambda i: (0, 0)),
+            in_vmem(), in_vmem(), in_vmem(),
         ],
         out_shape=[
             jax.ShapeDtypeStruct(sr.shape, f32),
@@ -206,8 +212,12 @@
             jax.ShapeDtypeStruct((out_rows, part), bf16),
         ],
         scratch_shapes=[pltpu.VMEM((cb, wb), bf16)] * 4 + [pltpu.VMEM((seq, model), f32)] * 2,
+        compiler_params=pltpu.CompilerParams(vmem_limit_bytes=24 << 20),
         name="mixer",
-    )(u, sr, si, decay, freq, log_step, inr, ini, cr, ci, skip, gv, gg, res, mix, gain, routes)
+    )(*map(
+        in_hbm,
+        (u, sr, si, decay, freq, log_step, inr, ini, cr, ci, skip, gv, gg, res, mix, gain, routes),
+    ))
 
 
 def swap_matrix(back):
@@ -217,39 +227,52 @@
     return jnp.where(source == j, 1.0, 0.0).astype(bf16)
 
 
-def expert_kernel(y_ref, wg_ref, wu_ref, wd_ref, z_ref):
+def expert_kernel(y_ref, wg_ref, wu_ref, wd_ref, z_ref, x_ref, h_ref, held, sems):
     model = wg_ref.shape[0]
     part = model // PARTS
     take = CHUNK // PARTS
     order = swap_matrix(False)
-    pieces = []
-    for c in range(y_ref.shape[0] // CHUNK):
+    chunks = y_ref.shape[0] // CHUNK
+    for c in range(chunks):
         x = dot(order, y_ref[CHUNK * c : CHUNK * (c + 1), :]).astype(bf16)
-        pieces.append(
-            jnp.concatenate([x[take * q : take * (q + 1)] for q in range(PARTS)], axis=1)
-        )
-    x = jnp.concatenate(pieces, axis=0)
-    gate = dot(x, wg_ref[...])
-    up = dot(x, wu_ref[...])
-    hidden = (gate * jax.nn.sigmoid(gate) * up).astype(bf16)
-    out = dot(hidden, wd_ref[...]).astype(bf16)
+        for q in range(PARTS):
+            x_ref[take * c : take * (c + 1), part * q : part * (q + 1)] = x[take * q : take * (q + 1)]
+    gate = dot(x_ref[...], wg_ref[...])
+    up = dot(x_ref[...], wu_ref[...])
+    h_ref[...] = (gate * jax.nn.sigmoid(gate) * up).astype(bf16)
     back = swap_matrix(True)
-    for c in range(y_ref.shape[0] // CHUNK):
-        o = out[take * c : take * (c + 1)]
-        o = jnp.concatenate([o[:, part * q : part * (q + 1)] for q in range(PARTS)], axis=0)
-        z_ref[CHUNK * c : CHUNK * (c + 1), :] = dot(back, o).astype(bf16)
+    halves = sems.shape[0]
+    rows = h_ref.shape[0] // halves
+    copies = []
+    for h in range(halves):
+        out = dot(h_ref[rows * h : rows * (h + 1), :], wd_ref[...]).astype(bf16)
+        for c in range(rows // take):
+            o = out[take * c : take * (c + 1)]
+            o = jnp.concatenate([o[:, part * q : part * (q + 1)] for q in range(PARTS)], axis=0)
+            first = PARTS * rows * h + CHUNK * c
+            held[first : first + CHUNK, :] = dot(back, o).astype(bf16)
+        span = pl.ds(PARTS * rows * h, PARTS * rows)
+        copy = pltpu.make_async_copy(held.at[span], z_ref.at[span], sems.at[h])
+        copy.start()
+        copies.append(copy)
+    for copy in copies:
+        copy.wait()
 
 
 def run_expert(y, wg, wu, wd):
-    steps = 4
-    whole = lambda x: pl.BlockSpec(x.shape, lambda i: (0, 0))
-    block = pl.BlockSpec((y.shape[0] // steps, y.shape[1]), lambda i: (i, 0))
+    rows = y.shape[0] // PARTS
     return pl.pallas_call(
         expert_kernel,
-        grid=(steps,),
-        in_specs=[block, whole(wg), whole(wu), whole(wd)],
-        out_specs=block,
-        out_shape=jax.ShapeDtypeStruct(y.shape, bf16),
+        in_specs=[in_vmem()] * 4,
+        out_specs=pl.BlockSpec(memory_space=pltpu.HBM),
+        out_shape=pltpu.HBM(y.shape, bf16),
+        scratch_shapes=[
+            pltpu.VMEM((rows, wg.shape[0]), bf16),
+            pltpu.VMEM((rows, wg.shape[1]), bf16),
+            pltpu.VMEM(y.shape, bf16),
+            pltpu.SemaphoreType.DMA((2,)),
+        ],
+        compiler_params=pltpu.CompilerParams(vmem_limit_bytes=20 << 20),
         name="expert",
     )(y, wg, wu, wd)
 
@@ -273,12 +296,12 @@
     weight = jnp.concatenate([weight] * PARTS, axis=1)
     hi, lo = split(weight)
     want = slot_pattern(seq)
-    for c in range(mix_ref.shape[0] // CHUNK):
+    for c in range(mix_ref.shape[1] // CHUNK):
         r = slice(16 * c, 16 * (c + 1))
         hit = spread_rows(code[r]) == want
         for h, w in enumerate((hi, lo)):
-            mix_ref[CHUNK * c : CHUNK * (c + 1), PARTS * seq * h : PARTS * seq * (h + 1)] = (
-                jnp.where(hit, spread_rows(w[r]), 0.0).astype(bf16)
+            mix_ref[PARTS * seq * h : PARTS * seq * (h + 1), CHUNK * c : CHUNK * (c + 1)] = (
+                jnp.where(hit, spread_rows(w[r]), 0.0).T.astype(bf16)
             )
 
 
@@ -288,8 +311,11 @@
         shared_kernel,
         out_shape=[
             jax.ShapeDtypeStruct((seq, model), f32),
-            jax.ShapeDtypeStruct((128 * CAPACITY * PARTS, 2 * PARTS * seq), bf16),
-        ],
+            pltpu.VMEM((2 * PARTS * seq, 128 * CAPACITY * PARTS), bf16),
+        ],
+        in_specs=[in_vmem()] * 6,
+        out_specs=[in_vmem()] * 2,
+        compiler_params=pltpu.CompilerParams(vmem_limit_bytes=16 << 20),
         cost_estimate=pl.CostEstimate(
             flops=2 * seq * model * wg.shape[1] * 60, bytes_accessed=8 << 20, transcendentals=0
         ),
@@ -299,9 +325,7 @@
 
 def combine_kernel(z_ref, mix_ref, shared_ref, mid_ref, gain_ref, out_ref):
     seq = mid_ref.shape[0]
-    both = lax.dot_general(
-        mix_ref[...], z_ref[...], (((0,), (0,)), ((), ())), preferred_element_type=f32
-    )
+    both = dot(mix_ref[...], z_ref[...])
     both = both[: PARTS * seq] + both[PARTS * seq :]
     routed = jnp.concatenate([both[seq * q : seq * (q + 1)] for q in range(PARTS)], axis=1)
     combined = shared_ref[...] + routed
@@ -314,6 +338,9 @@
     return pl.pallas_call(
         combine_kernel,
         out_shape=jax.ShapeDtypeStruct(mid.shape, bf16),
+        in_specs=[in_vmem()] * 5,
+        out_specs=in_vmem(),
+        compiler_params=pltpu.CompilerParams(vmem_limit_bytes=16 << 20),
         name="combine",
     )(z, mix, shared, mid, gain)
 

time: 106 us -> 98.8 us (0.932)
  Pallas kernels: 33.6 us -> 21.8 us
  local copies, waits for them, and re-layouts: 1.31 us -> 7.71 us
  waiting for transfers between devices: 24 us -> 22 us
    unnamed x2 -> x22, local copies, waits for them, and re-layouts: 1.31 us -> 7.71 us
    pallas_call x1, Pallas kernels: 10.1 us -> 5.71 us  [run_expert(): pl.pallas_call(expert_kernel, in_specs=[in_vmem()] * 4, out_specs=pl.Bloc...]
    pallas_call x1, Pallas kernels: 6.59 us -> 2.45 us  [run_shared(): pl.pallas_call(shared_kernel, out_shape=[jax.ShapeDtypeStruct((seq, model...]
    pallas_call x1, Pallas kernels: 4.52 us -> 2.11 us  [run_combine(): pl.pallas_call(combine_kernel, out_shape=jax.ShapeDtypeStruct(mid.shape,...]
    all_to_all x1, waiting for transfers between devices: 24 us -> 22 us  [exchange(): lax.all_to_all(x, 'ep', split_axis=0, concat_axis=0, tiled=True)]
  transfers between devices with their start and end apart: 1 -> 1, of which waited for: 1 -> 1; matrix products, arithmetic and copies ran while one was open for 0% -> 0% of each run, Pallas kernels for 6% -> 2%
where the time goes in v2:
time: 98.8 us; the launch traced here: 98.4 us
  blocking collectives  41.7 us (42%)
  waiting for transfers between devices  22 us (22%)
  Pallas kernels  21.8 us (22%)
  local copies, waits for them, and re-layouts  7.71 us (8%)
  starting transfers between devices  4.42 us (4%)
    all_to_all x1, blocking collectives, exchange(): lax.all_to_all(x, 'ep', split_axis=0, concat_axis=0, tiled=True)  41.7 us
    all_to_all x1, waiting for transfers between devices, exchange(): lax.all_to_all(x, 'ep', split_axis=0, concat_axis=0, tiled=True)  22 us
    pallas_call x1, Pallas kernels, run_mixer(): pl.pallas_call(mixer_kernel, grid=(steps,), in_specs=[cols(cb), cols(wb),...  11.5 us
    unnamed x22, local copies, waits for them, and re-layouts  7.71 us
    pallas_call x1, Pallas kernels, run_expert(): pl.pallas_call(expert_kernel, in_specs=[in_vmem()] * 4, out_specs=pl.Bloc...  5.71 us
    all_to_all x1, starting transfers between devices, exchange(): lax.all_to_all(x, 'ep', split_axis=0, concat_axis=0, tiled=True)  4.42 us
    pallas_call x1, Pallas kernels, run_shared(): pl.pallas_call(shared_kernel, out_shape=[jax.ShapeDtypeStruct((seq, model...  2.45 us
    pallas_call x1, Pallas kernels, run_combine(): pl.pallas_call(combine_kernel, out_shape=jax.ShapeDtypeStruct(mid.shape,...  2.11 us
  transfers between devices with their start and end apart: 1, of which 1 were waited for; matrix products, arithmetic and copies ran while one was open for 0% of the time, Pallas kernels for 2%

profile of v2, /device:TPU:1, one launch (start us, length us, event | category | flops | bytes accessed | tf_op | source)
XLA Modules:
  0.0 98.4 jit_solution(15554662138660659773)
XLA Ops:
  0.6 0.0 copy-start.2
  0.6 11.5 %mixer.1 = (f32[64,4096]{1,0:T(8,128)}, f32[64,4096]{1,0:T(8,128)}, bf16[64,2048]{1,0:T(8,128)(2,1)S(1)}, bf16[64,2048]{1,0:T(8,128)(2,1)S(1)}, bf16[2048,512]{1,0:T(8,128)(2,1)S(1)}) custom-call(bf16[64,1024]{1,0:T(8,128)(2,1)} %u_ref.1, f32[64,4096]{1,0:T(8,128)} %sr_ref.1, f32[64,4096]{1,0:T(8,128)} %si_ref.1, f32[64,64]{1,0:T(8,128)} %decay_ref.1, ...), custom_call_target="tpu_custom_call" | custom-call | tf_op jit(solution)/shard_map/mixer/pallas_call | solution.py:194
  12.2 0.0 copy-start
  12.2 0.0 copy-start.1
  12.2 41.7 %all_to_all.10 = bf16[128,16,512]{2,1,0:T(8,128)(2,1)S(1)} all-to-all(bf16[128,16,512]{2,1,0:T(8,128)(2,1)S(1)} %bitcast.27), channel_id=1, replica_groups=mesh['ep'=128] {'ep'}, dimensions={0} | all-to-all | bytes 4194304 | tf_op jit(solution)/shard_map/all_to_all | solution.py:371
  54.0 0.0 copy-done.2
  54.0 0.0 copy-done
  54.0 0.0 copy-done.1
  54.0 5.7 %expert.1 = bf16[2048,512]{1,0:T(8,128)(2,1)} custom-call(bf16[2048,512]{1,0:T(8,128)(2,1)S(1)} %bitcast.23, bf16[2048,512]{1,0:T(8,128)(2,1)S(1)} %bitcast.24, bf16[2048,512]{1,0:T(8,128)(2,1)S(1)} %bitcast.25, bf16[512,2048]{1,0:T(8,128)(2,1)S(1)} %bitcast.26), custom_call_target="tpu_custom_call" | custom-call | tf_op jit(solution)/shard_map/expert/pallas_call | solution.py:264
  59.7 0.0 copy-start.6
  59.7 0.0 copy-start.10
  59.7 4.4 %all-to-all-start.1 = ((bf16[128,16,512]{2,1,0:T(8,128)(2,1)}), bf16[128,16,512]{2,1,0:T(8,128)(2,1)S(1)}, u32[]{:S(2)}, u32[]{:S(2)}) async-start(bf16[128,16,512]{2,1,0:T(8,128)(2,1)} %bitcast.32), calls=%async_computation.1 | async-start | bytes 4194304 | tf_op jit(solution)/shard_map/all_to_all | solution.py:371
  64.1 0.0 copy-done.6
  64.1 0.0 copy-done.10
  64.2 0.0 copy-start.7
  64.2 1.6 %copy-done.7 = bf16[2048,512]{1,0:T(8,128)(2,1)S(1)} copy-done((bf16[2048,512]{1,0:T(8,128)(2,1)S(1)}, bf16[2048,512]{1,0:T(8,128)(2,1)}, u32[]{:S(2)}) %copy-start.7) | copy-done | bytes 2097176
  65.8 0.0 copy-start.8
  65.8 1.6 %copy-done.8 = bf16[2048,512]{1,0:T(8,128)(2,1)S(1)} copy-done((bf16[2048,512]{1,0:T(8,128)(2,1)S(1)}, bf16[2048,512]{1,0:T(8,128)(2,1)}, u32[]{:S(2)}) %copy-start.8) | copy-done | bytes 2097176
  67.3 0.0 copy-start.9
  67.3 1.6 %copy-done.9 = bf16[512,2048]{1,0:T(8,128)(2,1)S(1)} copy-done((bf16[512,2048]{1,0:T(8,128)(2,1)S(1)}, bf16[512,2048]{1,0:T(8,128)(2,1)}, u32[]{:S(2)}) %copy-start.9) | copy-done | bytes 2097176
  68.9 0.0 copy-start.5
  68.9 2.5 %shared.1 = (f32[64,2048]{1,0:T(8,128)S(1)}, bf16[512,2048]{1,0:T(8,128)(2,1)S(1)}) custom-call(bf16[64,2048]{1,0:T(8,128)(2,1)S(1)} %get-tuple-element.11.normed_ref, bf16[2048,512]{1,0:T(8,128)(2,1)S(1)} %copy-done.7, bf16[2048,512]{1,0:T(8,128)(2,1)S(1)} %copy-done.8, bf16[512,2048]{1,0:T(8,128)(2,1)S(1)} %copy-done.9, s32[6,64]{1,0:T(8,128)S(1)} %bitcast.30, ...), custom_call_target="tpu_custom_call" | custom-call | flops 8053063680 | bytes 8388608 | tf_op jit(solution)/shard_map/shared/pallas_call | solution.py:310
  71.4 0.0 copy-start.3
  71.4 1.3 %copy-done.3 = bf16[512,2048]{1,0:T(8,128)(2,1)} copy-done((bf16[512,2048]{1,0:T(8,128)(2,1)}, bf16[512,2048]{1,0:T(8,128)(2,1)S(1)}, u32[]{:S(2)}) %copy-start.3) | copy-done | bytes 2097176
  72.7 22.0 %all-to-all-done.1 = bf16[128,16,512]{2,1,0:T(8,128)(2,1)S(1)} async-done(((bf16[128,16,512]{2,1,0:T(8,128)(2,1)}), bf16[128,16,512]{2,1,0:T(8,128)(2,1)S(1)}, u32[]{:S(2)}, u32[]{:S(2)}) %all-to-all-start.1) | async-done | bytes 2097184 | tf_op jit(solution)/shard_map/all_to_all | solution.py:371
  94.7 0.0 copy-done.5
  94.7 0.0 copy-start.4
  94.7 1.6 %copy-done.4 = bf16[512,2048]{1,0:T(8,128)(2,1)S(1)} copy-done((bf16[512,2048]{1,0:T(8,128)(2,1)S(1)}, bf16[512,2048]{1,0:T(8,128)(2,1)}, u32[]{:S(2)}) %copy-start.4) | copy-done | bytes 2097176
  96.3 2.1 %combine.1 = bf16[64,2048]{1,0:T(8,128)(2,1)} custom-call(bf16[2048,512]{1,0:T(8,128)(2,1)S(1)} %bitcast.22, bf16[512,2048]{1,0:T(8,128)(2,1)S(1)} %copy-done.4, f32[64,2048]{1,0:T(8,128)S(1)} %get-tuple-element.13.shared_ref, bf16[64,2048]{1,0:T(8,128)(2,1)S(1)} %get-tuple-element.14.mid_ref, f32[1,2048]{1,0:T(1,128)S(1)} %bitcast.28), custom_call_target="tpu_custom_call" | custom-call | tf_op jit(solution)/shard_map/combine/pallas_call | solution.py:338
Async XLA Ops:
  0.6 53.3 %copy-start.2 = (bf16[1,512,2048]{2,1,0:T(8,128)(2,1)S(1)}, bf16[1,512,2048]{2,1,0:T(8,128)(2,1)}, u32[]{:S(2)}) copy-start(bf16[1,512,2048]{2,1,0:T(8,128)(2,1)} %param.46) | copy-start | bytes 6291460
  12.2 41.8 %copy-start = (bf16[1,2048,512]{2,1,0:T(8,128)(2,1)S(1)}, bf16[1,2048,512]{2,1,0:T(8,128)(2,1)}, u32[]{:S(2)}) copy-start(bf16[1,2048,512]{2,1,0:T(8,128)(2,1)} %param.44) | copy-start | bytes 6291460
  12.2 41.8 %copy-start.1 = (bf16[1,2048,512]{2,1,0:T(8,128)(2,1)S(1)}, bf16[1,2048,512]{2,1,0:T(8,128)(2,1)}, u32[]{:S(2)}) copy-start(bf16[1,2048,512]{2,1,0:T(8,128)(2,1)} %param.45) | copy-start | bytes 6291460
  59.7 4.5 %copy-start.6 = (s32[64,6]{0,1:T(8,128)S(1)}, s32[64,6]{0,1:T(8,128)}, u32[]{:S(2)}) copy-start(s32[64,6]{0,1:T(8,128)} %param.42) | copy-start | bytes 4612
  59.7 4.5 %copy-start.10 = (f32[64,6]{0,1:T(8,128)S(1)}, f32[64,6]{0,1:T(8,128)}, u32[]{:S(2)}) copy-start(f32[64,6]{0,1:T(8,128)} %param.43) | copy-start | bytes 4612
  59.7 35.0 %all-to-all-start.1 = ((bf16[128,16,512]{2,1,0:T(8,128)(2,1)}), bf16[128,16,512]{2,1,0:T(8,128)(2,1)S(1)}, u32[]{:S(2)}, u32[]{:S(2)}) async-start(bf16[128,16,512]{2,1,0:T(8,128)(2,1)} %bitcast.32), calls=%async_computation.1 | async-start | bytes 4194304 | tf_op jit(solution)/shard_map/all_to_all | solution.py:371
  64.2 1.6 %copy-start.7 = (bf16[2048,512]{1,0:T(8,128)(2,1)S(1)}, bf16[2048,512]{1,0:T(8,128)(2,1)}, u32[]{:S(2)}) copy-start(bf16[2048,512]{1,0:T(8,128)(2,1)} %wg_ref.1) | copy-start | bytes 6291460
  65.8 1.6 %copy-start.8 = (bf16[2048,512]{1,0:T(8,128)(2,1)S(1)}, bf16[2048,512]{1,0:T(8,128)(2,1)}, u32[]{:S(2)}) copy-start(bf16[2048,512]{1,0:T(8,128)(2,1)} %wu_ref.1) | copy-start | bytes 6291460
  67.3 1.6 %copy-start.9 = (bf16[512,2048]{1,0:T(8,128)(2,1)S(1)}, bf16[512,2048]{1,0:T(8,128)(2,1)}, u32[]{:S(2)}) copy-start(bf16[512,2048]{1,0:T(8,128)(2,1)} %wd_ref.1) | copy-start | bytes 6291460
  68.9 25.8 %copy-start.5 = (f32[2048]{0:T(1024)S(1)}, f32[2048]{0:T(1024)}, u32[]{:S(2)}) copy-start(f32[2048]{0:T(1024)} %param.41) | copy-start | bytes 24580
  71.4 1.3 %copy-start.3 = (bf16[512,2048]{1,0:T(8,128)(2,1)}, bf16[512,2048]{1,0:T(8,128)(2,1)S(1)}, u32[]{:S(2)}) copy-start(bf16[512,2048]{1,0:T(8,128)(2,1)S(1)} %get-tuple-element.12.mix_ref) | copy-start | bytes 6291460
  94.7 1.6 %copy-start.4 = (bf16[512,2048]{1,0:T(8,128)(2,1)S(1)}, bf16[512,2048]{1,0:T(8,128)(2,1)}, u32[]{:S(2)}) copy-start(bf16[512,2048]{1,0:T(8,128)(2,1)} %copy-done.3) | copy-start | bytes 6291460

commit v3 on v2

--- a/solution.py
+++ b/solution.py
@@ -73,30 +73,72 @@
     return lax.rsqrt(jnp.mean(x * x, axis=-1, keepdims=True) + norm_eps)
 
 
-def mixer_kernel(
-    u_ref, sr_ref, si_ref, decay_ref, freq_ref, log_ref, inr_ref, ini_ref, cr_ref, ci_ref,
-    skip_ref, gv_ref, gg_ref, res_ref, mix_ref, gain_ref, routes_ref,
-    nr_ref, ni_ref, mid_ref, normed_ref, out_ref,
-    br, bi, cr, ci, acc_v, acc_g,
-):
-    step = pl.program_id(0)
-    groups, states = decay_ref.shape
-    chans = inr_ref.shape[0] // groups
-    seq = u_ref.shape[0]
-    wide = groups * states
-
-    @pl.when(step == 0)
-    def _():
-        for ref in (br, bi, cr, ci):
-            ref[...] = jnp.zeros_like(ref)
-        acc_v[...] = jnp.zeros_like(acc_v)
-        acc_g[...] = jnp.zeros_like(acc_g)
-
-    logs = log_ref[...]
-    pick = iota((groups, logs.shape[1]), 1) == iota((groups, logs.shape[1]), 0) + step * groups
-    step_size = jnp.exp(jnp.sum(jnp.where(pick, logs, 0.0), axis=1, keepdims=True))
-    decay = decay_ref[...]
-    freq = freq_ref[...]
+MIXER_INS = 17
+
+
+def mixer_kernel(*refs):
+    hbm = refs[:MIXER_INS]
+    nr_ref, ni_ref, mid_ref, normed_ref, out_ref = refs[MIXER_INS : MIXER_INS + 5]
+    local = refs[MIXER_INS + 5 : 2 * MIXER_INS + 5]
+    nr, ni, select, small_sems, state_sems, glu_sems, out_sems = refs[2 * MIXER_INS + 5 :]
+    (u_v, sr, si, decay_v, freq_v, log_v, inr, ini, cr, ci,
+     skip_v, gv, gg, res_v, mix_v, gain_v, routes_v) = local
+
+    def copies_of(index, count, axis, sems, first):
+        size = hbm[index].shape[axis] // count
+        made = []
+        for k in range(count):
+            span = pl.ds(size * k, size)
+            at = (slice(None), span) if axis else (span, slice(None))
+            made.append(
+                pltpu.make_async_copy(hbm[index].at[at], local[index].at[at], sems.at[first + k])
+            )
+        return made
+
+    cuts = 4
+    small = {}
+    for n, index in enumerate((3, 4, 5, 16, 0, 6, 7, 8, 9, 10, 13, 14, 15)):
+        small[index] = copies_of(index, 1, 0, small_sems, n)[0]
+    state = [copies_of(1, cuts, 1, state_sems, 0), copies_of(2, cuts, 1, state_sems, cuts)]
+    value = copies_of(11, cuts, 0, glu_sems, 0)
+    gate = copies_of(12, cuts, 0, glu_sems, cuts)
+    for index in (3, 4, 5, 16, 0, 6, 7):
+        small[index].start()
+    for j in range(cuts):
+        state[0][j].start()
+        state[1][j].start()
+        if j == 0:
+            for index in (8, 9, 10):
+                small[index].start()
+    for copy in value:
+        copy.start()
+    for index in (13, 14, 15):
+        small[index].start()
+    for copy in gate:
+        copy.start()
+
+    seq = u_v.shape[0]
+    groups, states = decay_v.shape
+    packed = 4
+    wide = packed * states
+    cols = u_v.shape[1] // cuts
+    chans = cols // (groups // cuts)
+
+    small[16].wait()
+    code = route_code(routes_v[...])
+    code = jnp.concatenate([code] * PARTS, axis=1)
+    want = slot_pattern(seq)
+    for c in range(select.shape[0] // CHUNK):
+        here = spread_rows(code[16 * c : 16 * (c + 1)])
+        select[CHUNK * c : CHUNK * (c + 1), :] = jnp.where(here == want, 1.0, 0.0).astype(bf16)
+
+    small[5].wait()
+    small[3].wait()
+    small[4].wait()
+    pick = iota((groups, groups), 1) == iota((groups, groups), 0)
+    step_size = jnp.exp(jnp.sum(jnp.where(pick, log_v[...], 0.0), axis=1, keepdims=True))
+    decay = decay_v[...]
+    freq = freq_v[...]
     magnitude = jnp.exp(-decay * step_size)
     sin_x, cos_x = sin_cos(freq * step_size)
     a_re = magnitude * cos_x
@@ -106,68 +148,99 @@
     num = a_re - 1.0
     k_re = (num * lam + a_im * freq) / den
     k_im = (a_im * lam - num * freq) / den
-
-    lane_group = iota((groups, wide), 1) // states
-    own = iota((groups, wide), 0) == lane_group
+    own = iota((groups, wide), 0) % packed == iota((groups, wide), 1) // states
+
+    def tiled(x):
+        twice = jnp.concatenate([x, x], axis=1)
+        return jnp.concatenate([twice] * (packed // 2), axis=1)
 
     def flat(x):
-        twice = jnp.concatenate([x, x], axis=1)
-        tiled = jnp.concatenate([twice] * (groups // 2), axis=1)
-        return jnp.sum(jnp.where(own, tiled, 0.0), axis=0, keepdims=True)
+        x = jnp.where(own, tiled(x), 0.0)
+        return [
+            jnp.sum(x[packed * b : packed * (b + 1)], axis=0, keepdims=True)
+            for b in range(groups // packed)
+        ]
 
     a_re, a_im, k_re, k_im = flat(a_re), flat(a_im), flat(k_re), flat(k_im)
 
-    rows = groups * chans
-    patch = (iota((rows, 2 * states), 0) // chans) % 2 == iota((rows, 2 * states), 1) // states
-    for ref, src in ((br, inr_ref), (bi, ini_ref), (cr, cr_ref), (ci, ci_ref)):
-        x = src[...].astype(f32)
-        x = jnp.where(patch, jnp.concatenate([x, x], axis=1), 0.0).astype(bf16)
-        for j in range(groups // 2):
-            r = slice(2 * chans * j, 2 * chans * (j + 1))
-            ref[r, 2 * states * j : 2 * states * (j + 1)] = x[r]
-
-    u = u_ref[...]
-    f_re = dot(u, br[...])
-    f_im = dot(u, bi[...])
-    old_re = sr_ref[...]
-    old_im = si_ref[...]
-    new_re = a_re * old_re - a_im * old_im + (k_re * f_re - k_im * f_im)
-    new_im = a_re * old_im + a_im * old_re + (k_re * f_im + k_im * f_re)
-    nr_ref[...] = new_re
-    ni_ref[...] = new_im
-
-    def read(x, m):
-        hi, lo = split(x)
-        both = lax.dot_general(
-            jnp.concatenate([hi, lo], axis=0), m, (((1,), (1,)), ((), ())),
-            preferred_element_type=f32,
-        )
-        return both[:seq] + both[seq:]
-
-    mixed = read(new_re, cr[...]) - read(new_im, ci[...]) + skip_ref[...] * u.astype(f32)
-    act = jax.nn.gelu(mixed).astype(bf16)
-    acc_v[...] += dot(act, gv_ref[...])
-    acc_g[...] += dot(act, gg_ref[...])
-
-    @pl.when(step == pl.num_programs(0) - 1)
-    def _():
-        branch = acc_v[...] * jax.nn.sigmoid(acc_g[...])
-        mid = (res_ref[...].astype(f32) + branch * rms_scale(branch) * mix_ref[...]).astype(bf16)
-        mid_ref[...] = mid
-        mid = mid.astype(f32)
-        normed = (mid * rms_scale(mid) * gain_ref[...]).astype(bf16)
-        normed_ref[...] = normed
-        part = normed.shape[1] // PARTS
-        stacked = jnp.concatenate(
-            [normed[:, part * q : part * (q + 1)] for q in range(PARTS)], axis=0
-        )
-        code = route_code(routes_ref[...])
-        code = jnp.concatenate([code] * PARTS, axis=1)
-        want = slot_pattern(seq)
-        for c in range(out_ref.shape[0] // CHUNK):
-            here = spread_rows(code[16 * c : 16 * (c + 1)])
-            select = jnp.where(here == want, 1.0, 0.0).astype(bf16)
-            out_ref[CHUNK * c : CHUNK * (c + 1), :] = dot(select, stacked).astype(bf16)
+    patch = (iota((cols, wide), 0) // chans) % packed == iota((cols, wide), 1) // states
+
+    def weights(ref, j):
+        x = ref[cols * j : cols * (j + 1), :].astype(f32)
+        return jnp.where(patch, tiled(x), 0.0).astype(bf16)
+
+    lane = iota((seq, cols), 1) // (cols // packed)
+    for index in (0, 6, 7):
+        small[index].wait()
+    outs = []
+    acts = []
+    for j in range(cuts):
+        u = u_v[:, cols * j : cols * (j + 1)].astype(f32)
+        spread = jnp.concatenate(
+            [jnp.where(lane == k, u, 0.0) for k in range(packed)], axis=0
+        ).astype(bf16)
+        f_re = dot(spread, weights(inr, j))
+        f_im = dot(spread, weights(ini, j))
+        state[0][j].wait()
+        state[1][j].wait()
+        fresh_re, fresh_im = [], []
+        for k in range(packed):
+            b = packed * j + k
+            at = slice(wide * b, wide * (b + 1))
+            r = slice(seq * k, seq * (k + 1))
+            old_re = sr[:, at]
+            old_im = si[:, at]
+            new_re = a_re[b] * old_re - a_im[b] * old_im + (k_re[b] * f_re[r] - k_im[b] * f_im[r])
+            new_im = a_re[b] * old_im + a_im[b] * old_re + (k_re[b] * f_im[r] + k_im[b] * f_re[r])
+            nr[:, at] = new_re
+            ni[:, at] = new_im
+            fresh_re.append(new_re)
+            fresh_im.append(new_im)
+        for n, (src, dst) in enumerate(((nr, nr_ref), (ni, ni_ref))):
+            at = (slice(None), pl.ds(packed * wide * j, packed * wide))
+            copy = pltpu.make_async_copy(src.at[at], dst.at[at], out_sems.at[cuts * n + j])
+            copy.start()
+            outs.append(copy)
+        if j == 0:
+            for index in (8, 9, 10):
+                small[index].wait()
+
+        def read(parts, ref):
+            pairs = [split(x) for x in parts]
+            rows = jnp.concatenate([p[0] for p in pairs] + [p[1] for p in pairs], axis=0)
+            got = lax.dot_general(
+                rows, weights(ref, j), (((1,), (1,)), ((), ())), preferred_element_type=f32
+            )
+            return got[: packed * seq] + got[packed * seq :]
+
+        both = read(fresh_re, cr) - read(fresh_im, ci)
+        readout = both[:seq]
+        for k in range(1, packed):
+            readout = jnp.where(lane == k, both[seq * k : seq * (k + 1)], readout)
+        mixed = readout + skip_v[:, cols * j : cols * (j + 1)] * u
+        acts.append(jax.nn.gelu(mixed).astype(bf16))
+
+    act = jnp.concatenate(acts, axis=1)
+    for copy in value:
+        copy.wait()
+    value_part = dot(act, gv[...])
+    for copy in gate:
+        copy.wait()
+    branch = value_part * jax.nn.sigmoid(dot(act, gg[...]))
+    for index in (13, 14, 15):
+        small[index].wait()
+    mid = (res_v[...].astype(f32) + branch * rms_scale(branch) * mix_v[...]).astype(bf16)
+    mid_ref[...] = mid
+    mid = mid.astype(f32)
+    normed = (mid * rms_scale(mid) * gain_v[...]).astype(bf16)
+    normed_ref[...] = normed
+    part = normed.shape[1] // PARTS
+    stacked = jnp.concatenate(
+        [normed[:, part * q : part * (q + 1)] for q in range(PARTS)], axis=0
+    )
+    out_ref[...] = dot(select[...], stacked).astype(bf16)
+    for copy in outs:
+        copy.wait()
 
 
 def in_hbm(x):
@@ -178,46 +251,35 @@
     return pl.BlockSpec(memory_space=pltpu.VMEM)
 
 
-def run_mixer(
-    u, sr, si, decay, freq, log_step, inr, ini, cr, ci, skip, gv, gg, res, mix, gain, routes
-):
-    seq, width = u.shape
-    model = res.shape[1]
-    steps = 4
-    groups, states = decay.shape
+def run_mixer(*operands):
+    seq, model = operands[13].shape
+    state = operands[1].shape
     part = model // PARTS
-    gb, cb, wb = groups // steps, width // steps, groups * states // steps
-    cols = lambda n: pl.BlockSpec((seq, n), lambda i: (0, i))
-    rows = lambda r, n: pl.BlockSpec((r, n), lambda i: (i, 0))
-    whole = lambda x: pl.BlockSpec(x.shape, lambda i: (0, 0))
     out_rows = 128 * CAPACITY * PARTS
     return pl.pallas_call(
         mixer_kernel,
-        grid=(steps,),
-        in_specs=[
-            cols(cb), cols(wb), cols(wb), rows(gb, states), rows(gb, states), whole(log_step),
-            rows(cb, states), rows(cb, states), rows(cb, states), rows(cb, states),
-            pl.BlockSpec((1, cb), lambda i: (0, i)),
-            rows(cb, model), rows(cb, model), whole(res), whole(mix), whole(gain), whole(routes),
-        ],
-        out_specs=[
-            cols(wb), cols(wb),
-            in_vmem(), in_vmem(), in_vmem(),
-        ],
+        in_specs=[pl.BlockSpec(memory_space=pltpu.HBM)] * MIXER_INS,
+        out_specs=[pl.BlockSpec(memory_space=pltpu.HBM)] * 2 + [in_vmem()] * 3,
         out_shape=[
-            jax.ShapeDtypeStruct(sr.shape, f32),
-            jax.ShapeDtypeStruct(si.shape, f32),
+            pltpu.HBM(state, f32),
+            pltpu.HBM(state, f32),
             jax.ShapeDtypeStruct((seq, model), bf16),
             jax.ShapeDtypeStruct((seq, model), bf16),
             jax.ShapeDtypeStruct((out_rows, part), bf16),
         ],
-        scratch_shapes=[pltpu.VMEM((cb, wb), bf16)] * 4 + [pltpu.VMEM((seq, model), f32)] * 2,
-        compiler_params=pltpu.CompilerParams(vmem_limit_bytes=24 << 20),
+        scratch_shapes=[pltpu.VMEM(x.shape, x.dtype) for x in operands]
+        + [
+            pltpu.VMEM(state, f32),
+            pltpu.VMEM(state, f32),
+            pltpu.VMEM((out_rows, PARTS * seq), bf16),
+            pltpu.SemaphoreType.DMA((13,)),
+            pltpu.SemaphoreType.DMA((8,)),
+            pltpu.SemaphoreType.DMA((8,)),
+            pltpu.SemaphoreType.DMA((8,)),
+        ],
+        compiler_params=pltpu.CompilerParams(vmem_limit_bytes=28 << 20),
         name="mixer",
-    )(*map(
-        in_hbm,
-        (u, sr, si, decay, freq, log_step, inr, ini, cr, ci, skip, gv, gg, res, mix, gain, routes),
-    ))
+    )(*map(in_hbm, operands))
 
 
 def swap_matrix(back):
@@ -292,17 +354,15 @@
     weight = jnp.zeros(code.shape, f32)
     for k in range(top):
         weight = weight + jnp.where(row == routes[k : k + 1, :], weights[k : k + 1, :], 0.0)
-    code = jnp.concatenate([code] * PARTS, axis=1)
-    weight = jnp.concatenate([weight] * PARTS, axis=1)
-    hi, lo = split(weight)
-    want = slot_pattern(seq)
+    code = jnp.concatenate([code, code], axis=1)
+    weight = jnp.concatenate(split(weight), axis=1)
+    slot = (iota((CHUNK, 2 * seq), 0) % CAPACITY).astype(f32)
     for c in range(mix_ref.shape[1] // CHUNK):
         r = slice(16 * c, 16 * (c + 1))
-        hit = spread_rows(code[r]) == want
-        for h, w in enumerate((hi, lo)):
-            mix_ref[PARTS * seq * h : PARTS * seq * (h + 1), CHUNK * c : CHUNK * (c + 1)] = (
-                jnp.where(hit, spread_rows(w[r]), 0.0).T.astype(bf16)
-            )
+        hit = spread_rows(code[r]) == slot
+        mix_ref[:, CHUNK * c : CHUNK * (c + 1)] = (
+            jnp.where(hit, spread_rows(weight[r]), 0.0).T.astype(bf16)
+        )
 
 
 def run_shared(normed, wg, wu, wd, routes, weights):
@@ -311,7 +371,7 @@
         shared_kernel,
         out_shape=[
             jax.ShapeDtypeStruct((seq, model), f32),
-            pltpu.VMEM((2 * PARTS * seq, 128 * CAPACITY * PARTS), bf16),
+            jax.ShapeDtypeStruct((2 * seq, 128 * CAPACITY * PARTS), bf16),
         ],
         in_specs=[in_vmem()] * 6,
         out_specs=[in_vmem()] * 2,
@@ -325,9 +385,17 @@
 
 def combine_kernel(z_ref, mix_ref, shared_ref, mid_ref, gain_ref, out_ref):
     seq = mid_ref.shape[0]
-    both = dot(mix_ref[...], z_ref[...])
-    both = both[: PARTS * seq] + both[PARTS * seq :]
-    routed = jnp.concatenate([both[seq * q : seq * (q + 1)] for q in range(PARTS)], axis=1)
+    mix = mix_ref[...]
+    part_of = (iota((1, mix.shape[1]), 1) // CAPACITY) % PARTS
+    rows = [mix * jnp.where(part_of == q, 1.0, 0.0).astype(bf16) for q in range(PARTS)]
+    both = dot(jnp.concatenate(rows, axis=0), z_ref[...])
+    routed = jnp.concatenate(
+        [
+            both[2 * seq * q : 2 * seq * q + seq] + both[2 * seq * q + seq : 2 * seq * (q + 1)]
+            for q in range(PARTS)
+        ],
+        axis=1,
+    )
     combined = shared_ref[...] + routed
     out_ref[...] = (
         mid_ref[...].astype(f32) + combined * rms_scale(combined) * gain_ref[...]

time: 98.8 us -> 93.7 us (0.948)
  Pallas kernels: 21.8 us -> 17.7 us
  local copies, waits for them, and re-layouts: 7.71 us -> 5.76 us
  waiting for transfers between devices: 22 us -> 23 us
    pallas_call x1, Pallas kernels: 11.5 us -> 8.04 us  [run_mixer(): pl.pallas_call(mixer_kernel, in_specs=[pl.BlockSpec(memory_space=pltpu.HB...]
    unnamed x22, local copies, waits for them, and re-layouts: 7.71 us -> 5.76 us
where the time goes in v3:
time: 93.7 us; the launch traced here: 93.4 us
  blocking collectives  41.8 us (45%)
  waiting for transfers between devices  23 us (25%)
  Pallas kernels  17.7 us (19%)
  local copies, waits for them, and re-layouts  5.76 us (6%)
  starting transfers between devices  4.42 us (5%)
    all_to_all x1, blocking collectives, exchange(): lax.all_to_all(x, 'ep', split_axis=0, concat_axis=0, tiled=True)  41.8 us
    all_to_all x1, waiting for transfers between devices, exchange(): lax.all_to_all(x, 'ep', split_axis=0, concat_axis=0, tiled=True)  23 us
    pallas_call x1, Pallas kernels, run_mixer(): pl.pallas_call(mixer_kernel, in_specs=[pl.BlockSpec(memory_space=pltpu.HB...  8.04 us
    unnamed x22, local copies, waits for them, and re-layouts  5.76 us
    pallas_call x1, Pallas kernels, run_expert(): pl.pallas_call(expert_kernel, in_specs=[in_vmem()] * 4, out_specs=pl.Bloc...  5.71 us
    all_to_all x1, starting transfers between devices, exchange(): lax.all_to_all(x, 'ep', split_axis=0, concat_axis=0, tiled=True)  4.42 us
    pallas_call x1, Pallas kernels, run_combine(): pl.pallas_call(combine_kernel, out_shape=jax.ShapeDtypeStruct(mid.shape,...  2.11 us
  transfers between devices with their start and end apart: 1, of which 1 were waited for; matrix products, arithmetic and copies ran while one was open for 0% of the time, Pallas kernels for 2%

profile of v3, /device:TPU:1, one launch (start us, length us, event | category | flops | bytes accessed | tf_op | source)
XLA Modules:
  0.0 93.4 jit_solution(18319495964516839993)
XLA Ops:
  0.6 0.0 copy-start.2
  0.6 8.0 %mixer.1 = (f32[64,4096]{1,0:T(8,128)}, f32[64,4096]{1,0:T(8,128)}, bf16[64,2048]{1,0:T(8,128)(2,1)S(1)}, bf16[64,2048]{1,0:T(8,128)(2,1)S(1)}, bf16[2048,512]{1,0:T(8,128)(2,1)S(1)}) custom-call(bf16[64,1024]{1,0:T(8,128)(2,1)} %refs_0_.1, f32[64,4096]{1,0:T(8,128)} %refs_1_.1, f32[64,4096]{1,0:T(8,128)} %refs_2_.1, f32[64,64]{1,0:T(8,128)} %refs_3_.1, ...), custom_call_target="tpu_custom_call" | custom-call | tf_op jit(solution)/shard_map/mixer/pallas_call | solution.py:259
  8.7 0.0 copy-start.8
  8.7 0.0 copy-start
  8.7 0.0 copy-start.1
  8.7 41.8 %all_to_all.10 = bf16[128,16,512]{2,1,0:T(8,128)(2,1)S(1)} all-to-all(bf16[128,16,512]{2,1,0:T(8,128)(2,1)S(1)} %bitcast.27), channel_id=1, replica_groups=mesh['ep'=128] {'ep'}, dimensions={0} | all-to-all | bytes 4194304 | tf_op jit(solution)/shard_map/all_to_all | solution.py:439
  50.5 0.0 copy-done.8
  50.5 0.0 copy-done.2
  50.5 0.0 copy-done
  50.5 0.0 copy-done.1
  50.5 5.7 %expert.1 = bf16[2048,512]{1,0:T(8,128)(2,1)} custom-call(bf16[2048,512]{1,0:T(8,128)(2,1)S(1)} %bitcast.22, bf16[2048,512]{1,0:T(8,128)(2,1)S(1)} %bitcast.24, bf16[2048,512]{1,0:T(8,128)(2,1)S(1)} %bitcast.25, bf16[512,2048]{1,0:T(8,128)(2,1)S(1)} %bitcast.26), custom_call_target="tpu_custom_call" | custom-call | tf_op jit(solution)/shard_map/expert/pallas_call | solution.py:326
  56.2 0.0 copy-start.4
  56.2 0.0 copy-start.10
  56.2 4.4 %all-to-all-start.1 = ((bf16[128,16,512]{2,1,0:T(8,128)(2,1)}), bf16[128,16,512]{2,1,0:T(8,128)(2,1)S(1)}, u32[]{:S(2)}, u32[]{:S(2)}) async-start(bf16[128,16,512]{2,1,0:T(8,128)(2,1)} %bitcast.32), calls=%async_computation.1 | async-start | bytes 4194304 | tf_op jit(solution)/shard_map/all_to_all | solution.py:439
  60.7 0.0 copy-done.4
  60.7 0.0 copy-done.10
  60.7 0.0 copy-start.5
  60.7 1.6 %copy-done.5 = bf16[2048,512]{1,0:T(8,128)(2,1)S(1)} copy-done((bf16[2048,512]{1,0:T(8,128)(2,1)S(1)}, bf16[2048,512]{1,0:T(8,128)(2,1)}, u32[]{:S(2)}) %copy-start.5) | copy-done | bytes 2097176
  62.3 0.0 copy-start.6
  62.3 1.6 %copy-done.6 = bf16[2048,512]{1,0:T(8,128)(2,1)S(1)} copy-done((bf16[2048,512]{1,0:T(8,128)(2,1)S(1)}, bf16[2048,512]{1,0:T(8,128)(2,1)}, u32[]{:S(2)}) %copy-start.6) | copy-done | bytes 2097176
  63.9 0.0 copy-start.7
  63.9 1.6 %copy-done.7 = bf16[512,2048]{1,0:T(8,128)(2,1)S(1)} copy-done((bf16[512,2048]{1,0:T(8,128)(2,1)S(1)}, bf16[512,2048]{1,0:T(8,128)(2,1)}, u32[]{:S(2)}) %copy-start.7) | copy-done | bytes 2097176
  65.5 0.0 copy-start.9
  65.5 0.9 %copy-done.9 = bf16[64,2048]{1,0:T(8,128)(2,1)S(1)} copy-done((bf16[64,2048]{1,0:T(8,128)(2,1)S(1)}, bf16[64,2048]{1,0:T(8,128)(2,1)}, u32[]{:S(2)}) %copy-start.9) | copy-done | bytes 262168
  66.4 0.0 copy-start.3
  66.4 1.9 %shared.1 = (f32[64,2048]{1,0:T(8,128)S(1)}, bf16[128,2048]{1,0:T(8,128)(2,1)S(1)}) custom-call(bf16[64,2048]{1,0:T(8,128)(2,1)S(1)} %copy-done.9, bf16[2048,512]{1,0:T(8,128)(2,1)S(1)} %copy-done.5, bf16[2048,512]{1,0:T(8,128)(2,1)S(1)} %copy-done.6, bf16[512,2048]{1,0:T(8,128)(2,1)S(1)} %copy-done.7, s32[6,64]{1,0:T(8,128)S(1)} %bitcast.30, ...), custom_call_target="tpu_custom_call" | custom-call | flops 8053063680 | bytes 8388608 | tf_op jit(solution)/shard_map/shared/pallas_call | solution.py:370
  68.3 23.0 %all-to-all-done.1 = bf16[128,16,512]{2,1,0:T(8,128)(2,1)S(1)} async-done(((bf16[128,16,512]{2,1,0:T(8,128)(2,1)}), bf16[128,16,512]{2,1,0:T(8,128)(2,1)S(1)}, u32[]{:S(2)}, u32[]{:S(2)}) %all-to-all-start.1) | async-done | bytes 2097184 | tf_op jit(solution)/shard_map/all_to_all | solution.py:439
  91.3 0.0 copy-done.3
  91.3 2.1 %combine.1 = bf16[64,2048]{1,0:T(8,128)(2,1)} custom-call(bf16[2048,512]{1,0:T(8,128)(2,1)S(1)} %bitcast.23, bf16[128,2048]{1,0:T(8,128)(2,1)S(1)} %get-tuple-element.12.mix_ref, f32[64,2048]{1,0:T(8,128)S(1)} %get-tuple-element.13.shared_ref, bf16[64,2048]{1,0:T(8,128)(2,1)S(1)} %get-tuple-element.14.mid_ref, f32[1,2048]{1,0:T(1,128)S(1)} %bitcast.28), custom_call_target="tpu_custom_call" | custom-call | tf_op jit(solution)/shard_map/combine/pallas_call | solution.py:406
Async XLA Ops:
  0.6 49.9 %copy-start.2 = (bf16[1,512,2048]{2,1,0:T(8,128)(2,1)S(1)}, bf16[1,512,2048]{2,1,0:T(8,128)(2,1)}, u32[]{:S(2)}) copy-start(bf16[1,512,2048]{2,1,0:T(8,128)(2,1)} %param.46) | copy-start | bytes 6291460
  8.7 41.8 %copy-start.8 = (bf16[64,2048]{1,0:T(8,128)(2,1)}, bf16[64,2048]{1,0:T(8,128)(2,1)S(1)}, u32[]{:S(2)}) copy-start(bf16[64,2048]{1,0:T(8,128)(2,1)S(1)} %get-tuple-element.11.normed_ref) | copy-start | bytes 786436
  8.7 41.8 %copy-start = (bf16[1,2048,512]{2,1,0:T(8,128)(2,1)S(1)}, bf16[1,2048,512]{2,1,0:T(8,128)(2,1)}, u32[]{:S(2)}) copy-start(bf16[1,2048,512]{2,1,0:T(8,128)(2,1)} %param.44) | copy-start | bytes 6291460
  8.7 41.8 %copy-start.1 = (bf16[1,2048,512]{2,1,0:T(8,128)(2,1)S(1)}, bf16[1,2048,512]{2,1,0:T(8,128)(2,1)}, u32[]{:S(2)}) copy-start(bf16[1,2048,512]{2,1,0:T(8,128)(2,1)} %param.45) | copy-start | bytes 6291460
  56.2 4.5 %copy-start.4 = (s32[64,6]{0,1:T(8,128)S(1)}, s32[64,6]{0,1:T(8,128)}, u32[]{:S(2)}) copy-start(s32[64,6]{0,1:T(8,128)} %param.42) | copy-start | bytes 4612
  56.2 4.5 %copy-start.10 = (f32[64,6]{0,1:T(8,128)S(1)}, f32[64,6]{0,1:T(8,128)}, u32[]{:S(2)}) copy-start(f32[64,6]{0,1:T(8,128)} %param.43) | copy-start | bytes 4612
  56.2 35.0 %all-to-all-start.1 = ((bf16[128,16,512]{2,1,0:T(8,128)(2,1)}), bf16[128,16,512]{2,1,0:T(8,128)(2,1)S(1)}, u32[]{:S(2)}, u32[]{:S(2)}) async-start(bf16[128,16,512]{2,1,0:T(8,128)(2,1)} %bitcast.32), calls=%async_computation.1 | async-start | bytes 4194304 | tf_op jit(solution)/shard_map/all_to_all | solution.py:439
  60.7 1.6 %copy-start.5 = (bf16[2048,512]{1,0:T(8,128)(2,1)S(1)}, bf16[2048,512]{1,0:T(8,128)(2,1)}, u32[]{:S(2)}) copy-start(bf16[2048,512]{1,0:T(8,128)(2,1)} %wg_ref.1) | copy-start | bytes 6291460
  62.3 1.6 %copy-start.6 = (bf16[2048,512]{1,0:T(8,128)(2,1)S(1)}, bf16[2048,512]{1,0:T(8,128)(2,1)}, u32[]{:S(2)}) copy-start(bf16[2048,512]{1,0:T(8,128)(2,1)} %wu_ref.1) | copy-start | bytes 6291460
  63.9 1.6 %copy-start.7 = (bf16[512,2048]{1,0:T(8,128)(2,1)S(1)}, bf16[512,2048]{1,0:T(8,128)(2,1)}, u32[]{:S(2)}) copy-start(bf16[512,2048]{1,0:T(8,128)(2,1)} %wd_ref.1) | copy-start | bytes 6291460
  65.5 0.9 %copy-start.9 = (bf16[64,2048]{1,0:T(8,128)(2,1)S(1)}, bf16[64,2048]{1,0:T(8,128)(2,1)}, u32[]{:S(2)}) copy-start(bf16[64,2048]{1,0:T(8,128)(2,1)} %copy-done.8) | copy-start | bytes 786436
  66.4 24.9 %copy-start.3 = (f32[2048]{0:T(1024)S(1)}, f32[2048]{0:T(1024)}, u32[]{:S(2)}) copy-start(f32[2048]{0:T(1024)} %param.41) | copy-start | bytes 24580

commit v4 on v3

--- a/solution.py
+++ b/solution.py
@@ -41,11 +41,6 @@
     return sin_x, cos_x
 
 
-def split(x):
-    hi = x.astype(bf16)
-    return hi, (x - hi.astype(f32)).astype(bf16)
-
-
 def route_code(routes):
     top, seq = routes.shape
     experts = 128
@@ -80,7 +75,7 @@
     hbm = refs[:MIXER_INS]
     nr_ref, ni_ref, mid_ref, normed_ref, out_ref = refs[MIXER_INS : MIXER_INS + 5]
     local = refs[MIXER_INS + 5 : 2 * MIXER_INS + 5]
-    nr, ni, select, small_sems, state_sems, glu_sems, out_sems = refs[2 * MIXER_INS + 5 :]
+    nr, ni, select, force_re, force_im, read_re, read_im, small_sems, state_sems, glu_sems, out_sems = refs[2 * MIXER_INS + 5 :]
     (u_v, sr, si, decay_v, freq_v, log_v, inr, ini, cr, ci,
      skip_v, gv, gg, res_v, mix_v, gain_v, routes_v) = local
 
@@ -100,22 +95,19 @@
     for n, index in enumerate((3, 4, 5, 16, 0, 6, 7, 8, 9, 10, 13, 14, 15)):
         small[index] = copies_of(index, 1, 0, small_sems, n)[0]
     state = [copies_of(1, cuts, 1, state_sems, 0), copies_of(2, cuts, 1, state_sems, cuts)]
-    value = copies_of(11, cuts, 0, glu_sems, 0)
-    gate = copies_of(12, cuts, 0, glu_sems, cuts)
-    for index in (3, 4, 5, 16, 0, 6, 7):
+    glu_cuts = glu_sems.shape[0] // 2
+    value = copies_of(11, glu_cuts, 1, glu_sems, 0)
+    gate = copies_of(12, glu_cuts, 1, glu_sems, glu_cuts)
+    for index in (3, 4, 5, 16, 0, 6, 7, 8, 9, 10):
         small[index].start()
     for j in range(cuts):
         state[0][j].start()
         state[1][j].start()
-        if j == 0:
-            for index in (8, 9, 10):
-                small[index].start()
-    for copy in value:
-        copy.start()
+    for n in range(glu_cuts):
+        value[n].start()
+        gate[n].start()
     for index in (13, 14, 15):
         small[index].start()
-    for copy in gate:
-        copy.start()
 
     seq = u_v.shape[0]
     groups, states = decay_v.shape
@@ -172,15 +164,25 @@
     lane = iota((seq, cols), 1) // (cols // packed)
     for index in (0, 6, 7):
         small[index].wait()
-    outs = []
-    acts = []
     for j in range(cuts):
         u = u_v[:, cols * j : cols * (j + 1)].astype(f32)
         spread = jnp.concatenate(
             [jnp.where(lane == k, u, 0.0) for k in range(packed)], axis=0
         ).astype(bf16)
-        f_re = dot(spread, weights(inr, j))
-        f_im = dot(spread, weights(ini, j))
+        force_re[j] = dot(spread, weights(inr, j))
+        force_im[j] = dot(spread, weights(ini, j))
+    for index in (8, 9, 10):
+        small[index].wait()
+    for j in range(cuts):
+        read_re[j] = weights(cr, j)
+        read_im[j] = weights(ci, j)
+
+    outs = []
+    acts = []
+    for j in range(cuts):
+        u = u_v[:, cols * j : cols * (j + 1)].astype(f32)
+        f_re = force_re[j]
+        f_im = force_im[j]
         state[0][j].wait()
         state[1][j].wait()
         fresh_re, fresh_im = [], []
@@ -199,21 +201,15 @@
         for n, (src, dst) in enumerate(((nr, nr_ref), (ni, ni_ref))):
             at = (slice(None), pl.ds(packed * wide * j, packed * wide))
             copy = pltpu.make_async_copy(src.at[at], dst.at[at], out_sems.at[cuts * n + j])
-            copy.start()
             outs.append(copy)
-        if j == 0:
-            for index in (8, 9, 10):
-                small[index].wait()
 
         def read(parts, ref):
-            pairs = [split(x) for x in parts]
-            rows = jnp.concatenate([p[0] for p in pairs] + [p[1] for p in pairs], axis=0)
-            got = lax.dot_general(
-                rows, weights(ref, j), (((1,), (1,)), ((), ())), preferred_element_type=f32
+            rows = jnp.concatenate([x.astype(bf16) for x in parts], axis=0)
+            return lax.dot_general(
+                rows, ref[j], (((1,), (1,)), ((), ())), preferred_element_type=f32
             )
-            return got[: packed * seq] + got[packed * seq :]
-
-        both = read(fresh_re, cr) - read(fresh_im, ci)
+
+        both = read(fresh_re, read_re) - read(fresh_im, read_im)
         readout = both[:seq]
         for k in range(1, packed):
             readout = jnp.where(lane == k, both[seq * k : seq * (k + 1)], readout)
@@ -221,12 +217,18 @@
         acts.append(jax.nn.gelu(mixed).astype(bf16))
 
     act = jnp.concatenate(acts, axis=1)
-    for copy in value:
-        copy.wait()
-    value_part = dot(act, gv[...])
-    for copy in gate:
-        copy.wait()
-    branch = value_part * jax.nn.sigmoid(dot(act, gg[...]))
+    piece = gv.shape[1] // glu_cuts
+    pieces = []
+    for n in range(glu_cuts):
+        at = slice(piece * n, piece * (n + 1))
+        value[n].wait()
+        value_part = dot(act, gv[:, at])
+        gate[n].wait()
+        if n == glu_cuts - 1:
+            for copy in outs:
+                copy.start()
+        pieces.append(value_part * jax.nn.sigmoid(dot(act, gg[:, at])))
+    branch = jnp.concatenate(pieces, axis=1)
     for index in (13, 14, 15):
         small[index].wait()
     mid = (res_v[...].astype(f32) + branch * rms_scale(branch) * mix_v[...]).astype(bf16)
@@ -272,9 +274,13 @@
             pltpu.VMEM(state, f32),
             pltpu.VMEM(state, f32),
             pltpu.VMEM((out_rows, PARTS * seq), bf16),
+            pltpu.VMEM((4, 256, 256), f32),
+            pltpu.VMEM((4, 256, 256), f32),
+            pltpu.VMEM((4, 256, 256), bf16),
+            pltpu.VMEM((4, 256, 256), bf16),
             pltpu.SemaphoreType.DMA((13,)),
             pltpu.SemaphoreType.DMA((8,)),
-            pltpu.SemaphoreType.DMA((8,)),
+            pltpu.SemaphoreType.DMA((2,)),
             pltpu.SemaphoreType.DMA((8,)),
         ],
         compiler_params=pltpu.CompilerParams(vmem_limit_bytes=28 << 20),
@@ -303,7 +309,7 @@
     up = dot(x_ref[...], wu_ref[...])
     h_ref[...] = (gate * jax.nn.sigmoid(gate) * up).astype(bf16)
     back = swap_matrix(True)
-    halves = sems.shape[0]
+    halves = 2
     rows = h_ref.shape[0] // halves
     copies = []
     for h in range(halves):
@@ -313,10 +319,10 @@
             o = jnp.concatenate([o[:, part * q : part * (q + 1)] for q in range(PARTS)], axis=0)
             first = PARTS * rows * h + CHUNK * c
             held[first : first + CHUNK, :] = dot(back, o).astype(bf16)
-        span = pl.ds(PARTS * rows * h, PARTS * rows)
-        copy = pltpu.make_async_copy(held.at[span], z_ref.at[span], sems.at[h])
-        copy.start()
-        copies.append(copy)
+            span = pl.ds(first, CHUNK)
+            copy = pltpu.make_async_copy(held.at[span], z_ref.at[span], sems.at[first // CHUNK])
+            copy.start()
+            copies.append(copy)
     for copy in copies:
         copy.wait()
 
@@ -332,7 +338,7 @@
             pltpu.VMEM((rows, wg.shape[0]), bf16),
             pltpu.VMEM((rows, wg.shape[1]), bf16),
             pltpu.VMEM(y.shape, bf16),
-            pltpu.SemaphoreType.DMA((2,)),
+            pltpu.SemaphoreType.DMA((y.shape[0] // CHUNK,)),
         ],
         compiler_params=pltpu.CompilerParams(vmem_limit_bytes=20 << 20),
         name="expert",
@@ -354,9 +360,7 @@
     weight = jnp.zeros(code.shape, f32)
     for k in range(top):
         weight = weight + jnp.where(row == routes[k : k + 1, :], weights[k : k + 1, :], 0.0)
-    code = jnp.concatenate([code, code], axis=1)
-    weight = jnp.concatenate(split(weight), axis=1)
-    slot = (iota((CHUNK, 2 * seq), 0) % CAPACITY).astype(f32)
+    slot = (iota((CHUNK, seq), 0) % CAPACITY).astype(f32)
     for c in range(mix_ref.shape[1] // CHUNK):
         r = slice(16 * c, 16 * (c + 1))
         hit = spread_rows(code[r]) == slot
@@ -371,7 +375,7 @@
         shared_kernel,
         out_shape=[
             jax.ShapeDtypeStruct((seq, model), f32),
-            jax.ShapeDtypeStruct((2 * seq, 128 * CAPACITY * PARTS), bf16),
+            jax.ShapeDtypeStruct((seq, 128 * CAPACITY * PARTS), bf16),
         ],
         in_specs=[in_vmem()] * 6,
         out_specs=[in_vmem()] * 2,
@@ -389,13 +393,7 @@
     part_of = (iota((1, mix.shape[1]), 1) // CAPACITY) % PARTS
     rows = [mix * jnp.where(part_of == q, 1.0, 0.0).astype(bf16) for q in range(PARTS)]
     both = dot(jnp.concatenate(rows, axis=0), z_ref[...])
-    routed = jnp.concatenate(
-        [
-            both[2 * seq * q : 2 * seq * q + seq] + both[2 * seq * q + seq : 2 * seq * (q + 1)]
-            for q in range(PARTS)
-        ],
-        axis=1,
-    )
+    routed = jnp.concatenate([both[seq * q : seq * (q + 1)] for q in range(PARTS)], axis=1)
     combined = shared_ref[...] + routed
     out_ref[...] = (
         mid_ref[...].astype(f32) + combined * rms_scale(combined) * gain_ref[...]

time: 93.7 us -> 91.9 us (0.981)
  Pallas kernels: 17.7 us -> 15.8 us
  waiting for transfers between devices: 23 us -> 24 us
  local copies, waits for them, and re-layouts: 5.76 us -> 4.8 us
    pallas_call x1, Pallas kernels: 8.04 us -> 6.91 us  [run_mixer(): pl.pallas_call(mixer_kernel, in_specs=[pl.BlockSpec(memory_space=pltpu.HB...]
    all_to_all x1, waiting for transfers between devices: 23 us -> 24 us  [exchange(): lax.all_to_all(x, 'ep', split_axis=0, concat_axis=0, tiled=True)]
    unnamed x22 -> x18, local copies, waits for them, and re-layouts: 5.76 us -> 4.8 us
where the time goes in v4:
time: 91.9 us; the launch traced here: 91.6 us
  blocking collectives  41.8 us (45%)
  waiting for transfers between devices  24 us (26%)
  Pallas kernels  15.8 us (17%)
  local copies, waits for them, and re-layouts  4.8 us (5%)
  starting transfers between devices  4.42 us (5%)
    all_to_all x1, blocking collectives, exchange(): lax.all_to_all(x, 'ep', split_axis=0, concat_axis=0, tiled=True)  41.8 us
    all_to_all x1, waiting for transfers between devices, exchange(): lax.all_to_all(x, 'ep', split_axis=0, concat_axis=0, tiled=True)  24 us
    pallas_call x1, Pallas kernels, run_mixer(): pl.pallas_call(mixer_kernel, in_specs=[pl.BlockSpec(memory_space=pltpu.HB...  6.91 us
    pallas_call x1, Pallas kernels, run_expert(): pl.pallas_call(expert_kernel, in_specs=[in_vmem()] * 4, out_specs=pl.Bloc...  5.57 us
    unnamed x18, local copies, waits for them, and re-layouts  4.8 us
    all_to_all x1, starting transfers between devices, exchange(): lax.all_to_all(x, 'ep', split_axis=0, concat_axis=0, tiled=True)  4.42 us
  transfers between devices with their start and end apart: 1, of which 1 were waited for; matrix products, arithmetic and copies ran while one was open for 0% of the time, Pallas kernels for 2%

profile of v4, /device:TPU:1, one launch (start us, length us, event | category | flops | bytes accessed | tf_op | source)
XLA Modules:
  0.0 91.6 jit_solution(13313609927521417251)
XLA Ops:
  0.6 0.0 copy-start.2
  0.6 6.9 %mixer.1 = (f32[64,4096]{1,0:T(8,128)}, f32[64,4096]{1,0:T(8,128)}, bf16[64,2048]{1,0:T(8,128)(2,1)S(1)}, bf16[64,2048]{1,0:T(8,128)(2,1)S(1)}, bf16[2048,512]{1,0:T(8,128)(2,1)S(1)}) custom-call(bf16[64,1024]{1,0:T(8,128)(2,1)} %refs_0_.1, f32[64,4096]{1,0:T(8,128)} %refs_1_.1, f32[64,4096]{1,0:T(8,128)} %refs_2_.1, f32[64,64]{1,0:T(8,128)} %refs_3_.1, ...), custom_call_target="tpu_custom_call" | custom-call | tf_op jit(solution)/shard_map/mixer/pallas_call | solution.py:261
  7.6 0.0 copy-start
  7.6 0.0 copy-start.1
  7.6 41.8 %all_to_all.10 = bf16[128,16,512]{2,1,0:T(8,128)(2,1)S(1)} all-to-all(bf16[128,16,512]{2,1,0:T(8,128)(2,1)S(1)} %bitcast.27), channel_id=1, replica_groups=mesh['ep'=128] {'ep'}, dimensions={0} | all-to-all | bytes 4194304 | tf_op jit(solution)/shard_map/all_to_all | solution.py:437
  49.3 0.0 copy-done.2
  49.3 0.0 copy-done
  49.4 0.0 copy-done.1
  49.4 5.6 %expert.1 = bf16[2048,512]{1,0:T(8,128)(2,1)} custom-call(bf16[2048,512]{1,0:T(8,128)(2,1)S(1)} %bitcast.22, bf16[2048,512]{1,0:T(8,128)(2,1)S(1)} %bitcast.24, bf16[2048,512]{1,0:T(8,128)(2,1)S(1)} %bitcast.25, bf16[512,2048]{1,0:T(8,128)(2,1)S(1)} %bitcast.26), custom_call_target="tpu_custom_call" | custom-call | tf_op jit(solution)/shard_map/expert/pallas_call | solution.py:332
  54.9 0.0 copy-start.4
  54.9 0.0 copy-start.8
  55.0 4.4 %all-to-all-start.1 = ((bf16[128,16,512]{2,1,0:T(8,128)(2,1)}), bf16[128,16,512]{2,1,0:T(8,128)(2,1)S(1)}, u32[]{:S(2)}, u32[]{:S(2)}) async-start(bf16[128,16,512]{2,1,0:T(8,128)(2,1)} %bitcast.32), calls=%async_computation.1 | async-start | bytes 4194304 | tf_op jit(solution)/shard_map/all_to_all | solution.py:437
  59.4 0.0 copy-done.4
  59.4 0.0 copy-done.8
  59.4 0.0 copy-start.5
  59.4 1.6 %copy-done.5 = bf16[2048,512]{1,0:T(8,128)(2,1)S(1)} copy-done((bf16[2048,512]{1,0:T(8,128)(2,1)S(1)}, bf16[2048,512]{1,0:T(8,128)(2,1)}, u32[]{:S(2)}) %copy-start.5) | copy-done | bytes 2097176
  61.0 0.0 copy-start.6
  61.0 1.6 %copy-done.6 = bf16[2048,512]{1,0:T(8,128)(2,1)S(1)} copy-done((bf16[2048,512]{1,0:T(8,128)(2,1)S(1)}, bf16[2048,512]{1,0:T(8,128)(2,1)}, u32[]{:S(2)}) %copy-start.6) | copy-done | bytes 2097176
  62.6 0.0 copy-start.7
  62.6 1.6 %copy-done.7 = bf16[512,2048]{1,0:T(8,128)(2,1)S(1)} copy-done((bf16[512,2048]{1,0:T(8,128)(2,1)S(1)}, bf16[512,2048]{1,0:T(8,128)(2,1)}, u32[]{:S(2)}) %copy-start.7) | copy-done | bytes 2097176
  64.2 0.0 copy-start.3
  64.2 1.8 %shared.1 = (f32[64,2048]{1,0:T(8,128)S(1)}, bf16[64,2048]{1,0:T(8,128)(2,1)S(1)}) custom-call(bf16[64,2048]{1,0:T(8,128)(2,1)S(1)} %get-tuple-element.11.normed_ref, bf16[2048,512]{1,0:T(8,128)(2,1)S(1)} %copy-done.5, bf16[2048,512]{1,0:T(8,128)(2,1)S(1)} %copy-done.6, bf16[512,2048]{1,0:T(8,128)(2,1)S(1)} %copy-done.7, s32[6,64]{1,0:T(8,128)S(1)} %bitcast.30, ...), custom_call_target="tpu_custom_call" | custom-call | flops 8053063680 | bytes 8388608 | tf_op jit(solution)/shard_map/shared/pallas_call | solution.py:374
  66.0 24.0 %all-to-all-done.1 = bf16[128,16,512]{2,1,0:T(8,128)(2,1)S(1)} async-done(((bf16[128,16,512]{2,1,0:T(8,128)(2,1)}), bf16[128,16,512]{2,1,0:T(8,128)(2,1)S(1)}, u32[]{:S(2)}, u32[]{:S(2)}) %all-to-all-start.1) | async-done | bytes 2097184 | tf_op jit(solution)/shard_map/all_to_all | solution.py:437
  90.0 0.0 copy-done.3
  90.0 1.6 %combine.1 = bf16[64,2048]{1,0:T(8,128)(2,1)} custom-call(bf16[2048,512]{1,0:T(8,128)(2,1)S(1)} %bitcast.23, bf16[64,2048]{1,0:T(8,128)(2,1)S(1)} %get-tuple-element.12.mix_ref, f32[64,2048]{1,0:T(8,128)S(1)} %get-tuple-element.13.shared_ref, bf16[64,2048]{1,0:T(8,128)(2,1)S(1)} %get-tuple-element.14.mid_ref, f32[1,2048]{1,0:T(1,128)S(1)} %bitcast.28), custom_call_target="tpu_custom_call" | custom-call | tf_op jit(solution)/shard_map/combine/pallas_call | solution.py:404
Async XLA Ops:
  0.6 48.7 %copy-start.2 = (bf16[1,512,2048]{2,1,0:T(8,128)(2,1)S(1)}, bf16[1,512,2048]{2,1,0:T(8,128)(2,1)}, u32[]{:S(2)}) copy-start(bf16[1,512,2048]{2,1,0:T(8,128)(2,1)} %param.46) | copy-start | bytes 6291460
  7.6 41.8 %copy-start = (bf16[1,2048,512]{2,1,0:T(8,128)(2,1)S(1)}, bf16[1,2048,512]{2,1,0:T(8,128)(2,1)}, u32[]{:S(2)}) copy-start(bf16[1,2048,512]{2,1,0:T(8,128)(2,1)} %param.44) | copy-start | bytes 6291460
  7.6 41.8 %copy-start.1 = (bf16[1,2048,512]{2,1,0:T(8,128)(2,1)S(1)}, bf16[1,2048,512]{2,1,0:T(8,128)(2,1)}, u32[]{:S(2)}) copy-start(bf16[1,2048,512]{2,1,0:T(8,128)(2,1)} %param.45) | copy-start | bytes 6291460
  54.9 4.5 %copy-start.4 = (s32[64,6]{0,1:T(8,128)S(1)}, s32[64,6]{0,1:T(8,128)}, u32[]{:S(2)}) copy-start(s32[64,6]{0,1:T(8,128)} %param.42) | copy-start | bytes 4612
  54.9 4.5 %copy-start.8 = (f32[64,6]{0,1:T(8,128)S(1)}, f32[64,6]{0,1:T(8,128)}, u32[]{:S(2)}) copy-start(f32[64,6]{0,1:T(8,128)} %param.43) | copy-start | bytes 4612
  55.0 35.0 %all-to-all-start.1 = ((bf16[128,16,512]{2,1,0:T(8,128)(2,1)}), bf16[128,16,512]{2,1,0:T(8,128)(2,1)S(1)}, u32[]{:S(2)}, u32[]{:S(2)}) async-start(bf16[128,16,512]{2,1,0:T(8,128)(2,1)} %bitcast.32), calls=%async_computation.1 | async-start | bytes 4194304 | tf_op jit(solution)/shard_map/all_to_all | solution.py:437
  59.4 1.6 %copy-start.5 = (bf16[2048,512]{1,0:T(8,128)(2,1)S(1)}, bf16[2048,512]{1,0:T(8,128)(2,1)}, u32[]{:S(2)}) copy-start(bf16[2048,512]{1,0:T(8,128)(2,1)} %wg_ref.1) | copy-start | bytes 6291460
  61.0 1.6 %copy-start.6 = (bf16[2048,512]{1,0:T(8,128)(2,1)S(1)}, bf16[2048,512]{1,0:T(8,128)(2,1)}, u32[]{:S(2)}) copy-start(bf16[2048,512]{1,0:T(8,128)(2,1)} %wu_ref.1) | copy-start | bytes 6291460
  62.6 1.6 %copy-start.7 = (bf16[512,2048]{1,0:T(8,128)(2,1)S(1)}, bf16[512,2048]{1,0:T(8,128)(2,1)}, u32[]{:S(2)}) copy-start(bf16[512,2048]{1,0:T(8,128)(2,1)} %wd_ref.1) | copy-start | bytes 6291460
  64.2 25.8 %copy-start.3 = (f32[2048]{0:T(1024)S(1)}, f32[2048]{0:T(1024)}, u32[]{:S(2)}) copy-start(f32[2048]{0:T(1024)} %param.41) | copy-start | bytes 24580

commit v5 on v4

--- a/solution.py
+++ b/solution.py
@@ -11,9 +11,8 @@
 f32 = jnp.float32
 bf16 = jnp.bfloat16
 
-CHUNK = 256
+EXPERTS = 128
 CAPACITY = 4
-PARTS = 4
 
 
 def iota(shape, dim):
@@ -41,11 +40,15 @@
     return sin_x, cos_x
 
 
+def split(x):
+    hi = x.astype(bf16)
+    return hi, (x - hi.astype(f32)).astype(bf16)
+
+
 def route_code(routes):
     top, seq = routes.shape
-    experts = 128
-    row = iota((experts, seq), 0)
-    named = jnp.zeros((experts, seq), f32)
+    row = iota((EXPERTS, seq), 0)
+    named = jnp.zeros((EXPERTS, seq), f32)
     for k in range(top):
         named = named + jnp.where(row == routes[k : k + 1, :], 1.0, 0.0)
     before = jnp.where(iota((seq, seq), 0) < iota((seq, seq), 1), 1.0, 0.0).astype(bf16)
@@ -54,14 +57,13 @@
 
 
 def spread_rows(block):
-    one_hot = jnp.where(iota((CHUNK, 16), 0) // 16 == iota((CHUNK, 16), 1), 1.0, 0.0)
-    return dot(one_hot.astype(bf16), block.astype(bf16))
-
-
-def slot_pattern(seq):
-    i = iota((CHUNK, PARTS * seq), 0)
-    j = iota((CHUNK, PARTS * seq), 1)
-    return jnp.where((i // 4) % 4 == j // seq, (i % 4).astype(f32), -2.0)
+    n = block.shape[0]
+    one_hot = iota((CAPACITY * n, n), 0) // CAPACITY == iota((CAPACITY * n, n), 1)
+    return dot(jnp.where(one_hot, 1.0, 0.0).astype(bf16), block.astype(bf16))
+
+
+def slot_of_row(shape):
+    return (iota(shape, 0) % CAPACITY).astype(f32)
 
 
 def rms_scale(x):
@@ -117,12 +119,8 @@
     chans = cols // (groups // cuts)
 
     small[16].wait()
-    code = route_code(routes_v[...])
-    code = jnp.concatenate([code] * PARTS, axis=1)
-    want = slot_pattern(seq)
-    for c in range(select.shape[0] // CHUNK):
-        here = spread_rows(code[16 * c : 16 * (c + 1)])
-        select[CHUNK * c : CHUNK * (c + 1), :] = jnp.where(here == want, 1.0, 0.0).astype(bf16)
+    code = spread_rows(route_code(routes_v[...]))
+    select[...] = jnp.where(code == slot_of_row(code.shape), 1.0, 0.0).astype(bf16)
 
     small[5].wait()
     small[3].wait()
@@ -204,10 +202,12 @@
             outs.append(copy)
 
         def read(parts, ref):
-            rows = jnp.concatenate([x.astype(bf16) for x in parts], axis=0)
-            return lax.dot_general(
+            pairs = [split(x) for x in parts]
+            rows = jnp.concatenate([p[0] for p in pairs] + [p[1] for p in pairs], axis=0)
+            got = lax.dot_general(
                 rows, ref[j], (((1,), (1,)), ((), ())), preferred_element_type=f32
             )
+            return got[: packed * seq] + got[packed * seq :]
 
         both = read(fresh_re, read_re) - read(fresh_im, read_im)
         readout = both[:seq]
@@ -236,11 +236,11 @@
     mid = mid.astype(f32)
     normed = (mid * rms_scale(mid) * gain_v[...]).astype(bf16)
     normed_ref[...] = normed
-    part = normed.shape[1] // PARTS
-    stacked = jnp.concatenate(
-        [normed[:, part * q : part * (q + 1)] for q in range(PARTS)], axis=0
-    )
-    out_ref[...] = dot(select[...], stacked).astype(bf16)
+    width = 512
+    for n in range(normed.shape[1] // width):
+        at = slice(width * n, width * (n + 1))
+        rows = dot(select[...], normed[:, at]).astype(bf16)
+        out_ref[:, :, at] = rows.reshape(EXPERTS, CAPACITY, width)
     for copy in outs:
         copy.wait()
 
@@ -256,8 +256,6 @@
 def run_mixer(*operands):
     seq, model = operands[13].shape
     state = operands[1].shape
-    part = model // PARTS
-    out_rows = 128 * CAPACITY * PARTS
     return pl.pallas_call(
         mixer_kernel,
         in_specs=[pl.BlockSpec(memory_space=pltpu.HBM)] * MIXER_INS,
@@ -267,13 +265,13 @@
             pltpu.HBM(state, f32),
             jax.ShapeDtypeStruct((seq, model), bf16),
             jax.ShapeDtypeStruct((seq, model), bf16),
-            jax.ShapeDtypeStruct((out_rows, part), bf16),
+            jax.ShapeDtypeStruct((EXPERTS, CAPACITY, model), bf16),
         ],
         scratch_shapes=[pltpu.VMEM(x.shape, x.dtype) for x in operands]
         + [
             pltpu.VMEM(state, f32),
             pltpu.VMEM(state, f32),
-            pltpu.VMEM((out_rows, PARTS * seq), bf16),
+            pltpu.VMEM((EXPERTS * CAPACITY, seq), bf16),
             pltpu.VMEM((4, 256, 256), f32),
             pltpu.VMEM((4, 256, 256), f32),
             pltpu.VMEM((4, 256, 256), bf16),
@@ -288,61 +286,49 @@
     )(*map(in_hbm, operands))
 
 
-def swap_matrix(back):
-    i = iota((CHUNK, CHUNK), 1 if back else 0)
-    j = iota((CHUNK, CHUNK), 0 if back else 1)
-    source = ((i // 4) % 16) * 16 + (i // 64) * 4 + i % 4
-    return jnp.where(source == j, 1.0, 0.0).astype(bf16)
-
-
-def expert_kernel(y_ref, wg_ref, wu_ref, wd_ref, z_ref, x_ref, h_ref, held, sems):
-    model = wg_ref.shape[0]
-    part = model // PARTS
-    take = CHUNK // PARTS
-    order = swap_matrix(False)
-    chunks = y_ref.shape[0] // CHUNK
-    for c in range(chunks):
-        x = dot(order, y_ref[CHUNK * c : CHUNK * (c + 1), :]).astype(bf16)
-        for q in range(PARTS):
-            x_ref[take * c : take * (c + 1), part * q : part * (q + 1)] = x[take * q : take * (q + 1)]
+def expert_kernel(
+    y_ref, wg_ref, wu_ref, wd_hbm, z_ref, x_ref, h_ref, wd_ref, held, sems, wd_sem
+):
+    wd_copy = pltpu.make_async_copy(wd_hbm, wd_ref, wd_sem.at[0])
+    wd_copy.start()
+    senders, slots, model = y_ref.shape
+    x_ref[...] = y_ref[...].reshape(x_ref.shape)
     gate = dot(x_ref[...], wg_ref[...])
     up = dot(x_ref[...], wu_ref[...])
     h_ref[...] = (gate * jax.nn.sigmoid(gate) * up).astype(bf16)
-    back = swap_matrix(True)
-    halves = 2
-    rows = h_ref.shape[0] // halves
+    wd_copy.wait()
+    halves = sems.shape[0]
+    some = senders // halves
     copies = []
     for h in range(halves):
-        out = dot(h_ref[rows * h : rows * (h + 1), :], wd_ref[...]).astype(bf16)
-        for c in range(rows // take):
-            o = out[take * c : take * (c + 1)]
-            o = jnp.concatenate([o[:, part * q : part * (q + 1)] for q in range(PARTS)], axis=0)
-            first = PARTS * rows * h + CHUNK * c
-            held[first : first + CHUNK, :] = dot(back, o).astype(bf16)
-            span = pl.ds(first, CHUNK)
-            copy = pltpu.make_async_copy(held.at[span], z_ref.at[span], sems.at[first // CHUNK])
-            copy.start()
-            copies.append(copy)
+        out = dot(h_ref[slots * some * h : slots * some * (h + 1), :], wd_ref[...]).astype(bf16)
+        held[some * h : some * (h + 1)] = out.reshape(some, slots, model)
+        span = pl.ds(some * h, some)
+        copy = pltpu.make_async_copy(held.at[span], z_ref.at[span], sems.at[h])
+        copy.start()
+        copies.append(copy)
     for copy in copies:
         copy.wait()
 
 
 def run_expert(y, wg, wu, wd):
-    rows = y.shape[0] // PARTS
+    rows = y.shape[0] * y.shape[1]
     return pl.pallas_call(
         expert_kernel,
-        in_specs=[in_vmem()] * 4,
+        in_specs=[in_vmem()] * 3 + [pl.BlockSpec(memory_space=pltpu.HBM)],
         out_specs=pl.BlockSpec(memory_space=pltpu.HBM),
         out_shape=pltpu.HBM(y.shape, bf16),
         scratch_shapes=[
             pltpu.VMEM((rows, wg.shape[0]), bf16),
             pltpu.VMEM((rows, wg.shape[1]), bf16),
+            pltpu.VMEM(wd.shape, bf16),
             pltpu.VMEM(y.shape, bf16),
-            pltpu.SemaphoreType.DMA((y.shape[0] // CHUNK,)),
+            pltpu.SemaphoreType.DMA((2,)),
+            pltpu.SemaphoreType.DMA((1,)),
         ],
         compiler_params=pltpu.CompilerParams(vmem_limit_bytes=20 << 20),
         name="expert",
-    )(y, wg, wu, wd)
+    )(y, wg, wu, in_hbm(wd))
 
 
 def shared_kernel(normed_ref, wg_ref, wu_ref, wd_ref, routes_ref, weights_ref, out_ref, mix_ref):
@@ -360,13 +346,11 @@
     weight = jnp.zeros(code.shape, f32)
     for k in range(top):
         weight = weight + jnp.where(row == routes[k : k + 1, :], weights[k : k + 1, :], 0.0)
-    slot = (iota((CHUNK, seq), 0) % CAPACITY).astype(f32)
-    for c in range(mix_ref.shape[1] // CHUNK):
-        r = slice(16 * c, 16 * (c + 1))
-        hit = spread_rows(code[r]) == slot
-        mix_ref[:, CHUNK * c : CHUNK * (c + 1)] = (
-            jnp.where(hit, spread_rows(weight[r]), 0.0).T.astype(bf16)
-        )
+    code = spread_rows(code)
+    hit = code == slot_of_row(code.shape)
+    hi, lo = split(weight)
+    for h, w in enumerate((hi, lo)):
+        mix_ref[seq * h : seq * (h + 1), :] = jnp.where(hit, spread_rows(w), 0.0).T.astype(bf16)
 
 
 def run_shared(normed, wg, wu, wd, routes, weights):
@@ -375,7 +359,7 @@
         shared_kernel,
         out_shape=[
             jax.ShapeDtypeStruct((seq, model), f32),
-            jax.ShapeDtypeStruct((seq, 128 * CAPACITY * PARTS), bf16),
+            jax.ShapeDtypeStruct((2 * seq, EXPERTS * CAPACITY), bf16),
         ],
         in_specs=[in_vmem()] * 6,
         out_specs=[in_vmem()] * 2,
@@ -389,11 +373,8 @@
 
 def combine_kernel(z_ref, mix_ref, shared_ref, mid_ref, gain_ref, out_ref):
     seq = mid_ref.shape[0]
-    mix = mix_ref[...]
-    part_of = (iota((1, mix.shape[1]), 1) // CAPACITY) % PARTS
-    rows = [mix * jnp.where(part_of == q, 1.0, 0.0).astype(bf16) for q in range(PARTS)]
-    both = dot(jnp.concatenate(rows, axis=0), z_ref[...])
-    routed = jnp.concatenate([both[seq * q : seq * (q + 1)] for q in range(PARTS)], axis=1)
+    both = dot(mix_ref[...], z_ref[...].reshape(mix_ref.shape[1], out_ref.shape[1]))
+    routed = both[:seq] + both[seq:]
     combined = shared_ref[...] + routed
     out_ref[...] = (
         mid_ref[...].astype(f32) + combined * rms_scale(combined) * gain_ref[...]
@@ -418,8 +399,6 @@
     expert_down, shared_gate, shared_up, shared_down,
 ):
     states = decay_rate.shape[1]
-    model = residual.shape[1]
-    part = model // PARTS
     row = lambda v: v.reshape(1, -1)
     inr = jnp.transpose(input_real, (0, 2, 1)).reshape(-1, states)
     ini = jnp.transpose(input_imag, (0, 2, 1)).reshape(-1, states)
@@ -433,8 +412,7 @@
     )
 
     def exchange(x):
-        x = x.reshape(128, PARTS * CAPACITY, part)
-        return lax.all_to_all(x, "ep", split_axis=0, concat_axis=0, tiled=True).reshape(-1, part)
+        return lax.all_to_all(x, "ep", split_axis=0, concat_axis=0, tiled=True)
 
     arrived = exchange(outgoing)
     shared, mix = run_shared(normed, shared_gate, shared_up, shared_down, routes_t, weights_t)

time: 91.9 us -> 91.8 us (level)
    unnamed x18 -> x16, local copies, waits for them, and re-layouts: 4.8 us -> 4.8 us
where the time goes in v5:
time: 91.8 us; the launch traced here: 91.5 us
  blocking collectives  41.7 us (45%)
  waiting for transfers between devices  24.1 us (26%)
  Pallas kernels  15.7 us (17%)
  local copies, waits for them, and re-layouts  4.8 us (5%)
  starting transfers between devices  4.43 us (5%)
    all_to_all x1, blocking collectives, exchange(): return lax.all_to_all(x, 'ep', split_axis=0, concat_axis=0, tiled=True)  41.7 us
    all_to_all x1, waiting for transfers between devices, exchange(): return lax.all_to_all(x, 'ep', split_axis=0, concat_axis=0, tiled=True)  24.1 us
    pallas_call x1, Pallas kernels, run_mixer(): pl.pallas_call(mixer_kernel, in_specs=[pl.BlockSpec(memory_space=pltpu.HB...  6.77 us
    pallas_call x1, Pallas kernels, run_expert(): pl.pallas_call(expert_kernel, in_specs=[in_vmem()] * 3 + [pl.BlockSpec(me...  5.9 us
    unnamed x16, local copies, waits for them, and re-layouts  4.8 us
    all_to_all x1, starting transfers between devices, exchange(): return lax.all_to_all(x, 'ep', split_axis=0, concat_axis=0, tiled=True)  4.43 us
  transfers between devices with their start and end apart: 1, of which 1 were waited for; matrix products, arithmetic and copies ran while one was open for 0% of the time, Pallas kernels for 2%

profile of v5, /device:TPU:1, one launch (start us, length us, event | category | flops | bytes accessed | tf_op | source)
XLA Modules:
  0.0 91.5 jit_solution(10984883782740412270)
XLA Ops:
  0.6 6.8 %mixer.1 = (f32[64,4096]{1,0:T(8,128)}, f32[64,4096]{1,0:T(8,128)}, bf16[64,2048]{1,0:T(8,128)(2,1)S(1)}, bf16[64,2048]{1,0:T(8,128)(2,1)S(1)}, bf16[128,4,2048]{2,1,0:T(4,128)(2,1)S(1)}) custom-call(bf16[64,1024]{1,0:T(8,128)(2,1)} %refs_0_.1, f32[64,4096]{1,0:T(8,128)} %refs_1_.1, f32[64,4096]{1,0:T(8,128)} %refs_2_.1, f32[64,64]{1,0:T(8,128)} %refs_3_.1, ...), custom_call_target="tpu_custom_call" | custom-call | tf_op jit(solution)/shard_map/mixer/pallas_call | solution.py:259
  7.4 0.0 copy-start
  7.4 0.0 copy-start.1
  7.4 41.7 %all_to_all.10.y_ref = bf16[128,4,2048]{2,1,0:T(4,128)(2,1)S(1)} all-to-all(bf16[128,4,2048]{2,1,0:T(4,128)(2,1)S(1)} %get-tuple-element.10), channel_id=1, replica_groups=mesh['ep'=128] {'ep'}, dimensions={0} | all-to-all | bytes 4194304 | tf_op jit(solution)/shard_map/all_to_all | solution.py:415
  49.2 0.0 copy-done
  49.2 0.0 copy-done.1
  49.2 5.9 %expert.1 = bf16[128,4,2048]{2,1,0:T(4,128)(2,1)} custom-call(bf16[128,4,2048]{2,1,0:T(4,128)(2,1)S(1)} %all_to_all.10.y_ref, bf16[2048,512]{1,0:T(8,128)(2,1)S(1)} %bitcast.18, bf16[2048,512]{1,0:T(8,128)(2,1)S(1)} %bitcast.19, bf16[512,2048]{1,0:T(8,128)(2,1)} %bitcast.24), custom_call_target="tpu_custom_call" | custom-call | tf_op jit(solution)/shard_map/expert/pallas_call | solution.py:316
  55.1 0.0 copy-start.3
  55.1 0.0 copy-start.7
  55.1 4.4 %all-to-all-start.1 = ((bf16[128,4,2048]{2,1,0:T(4,128)(2,1)}), bf16[128,4,2048]{2,1,0:T(4,128)(2,1)S(1)}, u32[]{:S(2)}, u32[]{:S(2)}) async-start(bf16[128,4,2048]{2,1,0:T(4,128)(2,1)} %expert.1), calls=%async_computation.1 | async-start | bytes 4194304 | tf_op jit(solution)/shard_map/all_to_all | solution.py:415
  59.6 0.0 copy-done.3
  59.6 0.0 copy-done.7
  59.6 0.0 copy-start.4
  59.6 1.6 %copy-done.4 = bf16[2048,512]{1,0:T(8,128)(2,1)S(1)} copy-done((bf16[2048,512]{1,0:T(8,128)(2,1)S(1)}, bf16[2048,512]{1,0:T(8,128)(2,1)}, u32[]{:S(2)}) %copy-start.4) | copy-done | bytes 2097176
  61.2 0.0 copy-start.5
  61.2 1.6 %copy-done.5 = bf16[2048,512]{1,0:T(8,128)(2,1)S(1)} copy-done((bf16[2048,512]{1,0:T(8,128)(2,1)S(1)}, bf16[2048,512]{1,0:T(8,128)(2,1)}, u32[]{:S(2)}) %copy-start.5) | copy-done | bytes 2097176
  62.8 0.0 copy-start.6
  62.8 1.6 %copy-done.6 = bf16[512,2048]{1,0:T(8,128)(2,1)S(1)} copy-done((bf16[512,2048]{1,0:T(8,128)(2,1)S(1)}, bf16[512,2048]{1,0:T(8,128)(2,1)}, u32[]{:S(2)}) %copy-start.6) | copy-done | bytes 2097176
  64.4 0.0 copy-start.2
  64.4 1.7 %shared.1 = (f32[64,2048]{1,0:T(8,128)S(1)}, bf16[128,512]{1,0:T(8,128)(2,1)S(1)}) custom-call(bf16[64,2048]{1,0:T(8,128)(2,1)S(1)} %get-tuple-element.11.normed_ref, bf16[2048,512]{1,0:T(8,128)(2,1)S(1)} %copy-done.4, bf16[2048,512]{1,0:T(8,128)(2,1)S(1)} %copy-done.5, bf16[512,2048]{1,0:T(8,128)(2,1)S(1)} %copy-done.6, s32[6,64]{1,0:T(8,128)S(1)} %bitcast.22, ...), custom_call_target="tpu_custom_call" | custom-call | flops 8053063680 | bytes 8388608 | tf_op jit(solution)/shard_map/shared/pallas_call | solution.py:358
  66.1 24.1 %all-to-all-done.1.z_ref = bf16[128,4,2048]{2,1,0:T(4,128)(2,1)S(1)} async-done(((bf16[128,4,2048]{2,1,0:T(4,128)(2,1)}), bf16[128,4,2048]{2,1,0:T(4,128)(2,1)S(1)}, u32[]{:S(2)}, u32[]{:S(2)}) %all-to-all-start.1) | async-done | bytes 2097184 | tf_op jit(solution)/shard_map/all_to_all | solution.py:415
  90.2 0.0 copy-done.2
  90.2 1.3 %combine.1 = bf16[64,2048]{1,0:T(8,128)(2,1)} custom-call(bf16[128,4,2048]{2,1,0:T(4,128)(2,1)S(1)} %all-to-all-done.1.z_ref, bf16[128,512]{1,0:T(8,128)(2,1)S(1)} %get-tuple-element.12.mix_ref, f32[64,2048]{1,0:T(8,128)S(1)} %get-tuple-element.13.shared_ref, bf16[64,2048]{1,0:T(8,128)(2,1)S(1)} %get-tuple-element.14.mid_ref, f32[1,2048]{1,0:T(1,128)S(1)} %bitcast.20), custom_call_target="tpu_custom_call" | custom-call | tf_op jit(solution)/shard_map/combine/pallas_call | solution.py:385
Async XLA Ops:
  7.4 41.8 %copy-start = (bf16[1,2048,512]{2,1,0:T(8,128)(2,1)S(1)}, bf16[1,2048,512]{2,1,0:T(8,128)(2,1)}, u32[]{:S(2)}) copy-start(bf16[1,2048,512]{2,1,0:T(8,128)(2,1)} %param.44) | copy-start | bytes 6291460
  7.4 41.8 %copy-start.1 = (bf16[1,2048,512]{2,1,0:T(8,128)(2,1)S(1)}, bf16[1,2048,512]{2,1,0:T(8,128)(2,1)}, u32[]{:S(2)}) copy-start(bf16[1,2048,512]{2,1,0:T(8,128)(2,1)} %param.45) | copy-start | bytes 6291460
  55.1 4.5 %copy-start.3 = (s32[64,6]{0,1:T(8,128)S(1)}, s32[64,6]{0,1:T(8,128)}, u32[]{:S(2)}) copy-start(s32[64,6]{0,1:T(8,128)} %param.42) | copy-start | bytes 4612
  55.1 4.5 %copy-start.7 = (f32[64,6]{0,1:T(8,128)S(1)}, f32[64,6]{0,1:T(8,128)}, u32[]{:S(2)}) copy-start(f32[64,6]{0,1:T(8,128)} %param.43) | copy-start | bytes 4612
  55.1 35.0 %all-to-all-start.1 = ((bf16[128,4,2048]{2,1,0:T(4,128)(2,1)}), bf16[128,4,2048]{2,1,0:T(4,128)(2,1)S(1)}, u32[]{:S(2)}, u32[]{:S(2)}) async-start(bf16[128,4,2048]{2,1,0:T(4,128)(2,1)} %expert.1), calls=%async_computation.1 | async-start | bytes 4194304 | tf_op jit(solution)/shard_map/all_to_all | solution.py:415
  59.6 1.6 %copy-start.4 = (bf16[2048,512]{1,0:T(8,128)(2,1)S(1)}, bf16[2048,512]{1,0:T(8,128)(2,1)}, u32[]{:S(2)}) copy-start(bf16[2048,512]{1,0:T(8,128)(2,1)} %wg_ref.1) | copy-start | bytes 6291460
  61.2 1.6 %copy-start.5 = (bf16[2048,512]{1,0:T(8,128)(2,1)S(1)}, bf16[2048,512]{1,0:T(8,128)(2,1)}, u32[]{:S(2)}) copy-start(bf16[2048,512]{1,0:T(8,128)(2,1)} %wu_ref.1) | copy-start | bytes 6291460
  62.8 1.6 %copy-start.6 = (bf16[512,2048]{1,0:T(8,128)(2,1)S(1)}, bf16[512,2048]{1,0:T(8,128)(2,1)}, u32[]{:S(2)}) copy-start(bf16[512,2048]{1,0:T(8,128)(2,1)} %wd_ref.1) | copy-start | bytes 6291460
  64.4 25.8 %copy-start.2 = (f32[2048]{0:T(1024)S(1)}, f32[2048]{0:T(1024)}, u32[]{:S(2)}) copy-start(f32[2048]{0:T(1024)} %param.41) | copy-start | bytes 24580

commit v6 on v5

--- a/solution.py
+++ b/solution.py
@@ -286,25 +286,20 @@
     )(*map(in_hbm, operands))
 
 
-def expert_kernel(
-    y_ref, wg_ref, wu_ref, wd_hbm, z_ref, x_ref, h_ref, wd_ref, held, sems, wd_sem
-):
-    wd_copy = pltpu.make_async_copy(wd_hbm, wd_ref, wd_sem.at[0])
-    wd_copy.start()
+def expert_kernel(y_ref, wg_ref, wu_ref, wd_ref, z_ref, h_ref, held, sems):
     senders, slots, model = y_ref.shape
-    x_ref[...] = y_ref[...].reshape(x_ref.shape)
-    gate = dot(x_ref[...], wg_ref[...])
-    up = dot(x_ref[...], wu_ref[...])
+    x = y_ref[...].reshape(senders * slots, model)
+    gate = dot(x, wg_ref[...])
+    up = dot(x, wu_ref[...])
     h_ref[...] = (gate * jax.nn.sigmoid(gate) * up).astype(bf16)
-    wd_copy.wait()
-    halves = sems.shape[0]
-    some = senders // halves
+    pieces = sems.shape[0]
+    width = model // pieces
     copies = []
-    for h in range(halves):
-        out = dot(h_ref[slots * some * h : slots * some * (h + 1), :], wd_ref[...]).astype(bf16)
-        held[some * h : some * (h + 1)] = out.reshape(some, slots, model)
-        span = pl.ds(some * h, some)
-        copy = pltpu.make_async_copy(held.at[span], z_ref.at[span], sems.at[h])
+    for n in range(pieces):
+        out = dot(h_ref[...], wd_ref[:, width * n : width * (n + 1)]).astype(bf16)
+        held[:, :, width * n : width * (n + 1)] = out.reshape(senders, slots, width)
+        at = (slice(None), slice(None), pl.ds(width * n, width))
+        copy = pltpu.make_async_copy(held.at[at], z_ref.at[at], sems.at[n])
         copy.start()
         copies.append(copy)
     for copy in copies:
@@ -315,20 +310,17 @@
     rows = y.shape[0] * y.shape[1]
     return pl.pallas_call(
         expert_kernel,
-        in_specs=[in_vmem()] * 3 + [pl.BlockSpec(memory_space=pltpu.HBM)],
+        in_specs=[in_vmem()] * 4,
         out_specs=pl.BlockSpec(memory_space=pltpu.HBM),
         out_shape=pltpu.HBM(y.shape, bf16),
         scratch_shapes=[
-            pltpu.VMEM((rows, wg.shape[0]), bf16),
             pltpu.VMEM((rows, wg.shape[1]), bf16),
-            pltpu.VMEM(wd.shape, bf16),
             pltpu.VMEM(y.shape, bf16),
-            pltpu.SemaphoreType.DMA((2,)),
-            pltpu.SemaphoreType.DMA((1,)),
+            pltpu.SemaphoreType.DMA((4,)),
         ],
         compiler_params=pltpu.CompilerParams(vmem_limit_bytes=20 << 20),
         name="expert",
-    )(y, wg, wu, in_hbm(wd))
+    )(y, wg, wu, wd)
 
 
 def shared_kernel(normed_ref, wg_ref, wu_ref, wd_ref, routes_ref, weights_ref, out_ref, mix_ref):

time: 91.8 us -> 90.4 us (0.985)
  Pallas kernels: 15.7 us -> 14.2 us
    pallas_call x1, Pallas kernels: 5.9 us -> 4.3 us  [run_expert(): pl.pallas_call(expert_kernel, in_specs=[in_vmem()] * 4, out_specs=pl.Bloc...]
    unnamed x16 -> x18, local copies, waits for them, and re-layouts: 4.8 us -> 4.8 us
where the time goes in v6:
time: 90.4 us; the launch traced here: 90.1 us
  blocking collectives  41.8 us (46%)
  waiting for transfers between devices  24.1 us (27%)
  Pallas kernels  14.2 us (16%)
  local copies, waits for them, and re-layouts  4.8 us (5%)
  starting transfers between devices  4.42 us (5%)
    all_to_all x1, blocking collectives, exchange(): return lax.all_to_all(x, 'ep', split_axis=0, concat_axis=0, tiled=True)  41.8 us
    all_to_all x1, waiting for transfers between devices, exchange(): return lax.all_to_all(x, 'ep', split_axis=0, concat_axis=0, tiled=True)  24.1 us
    pallas_call x1, Pallas kernels, run_mixer(): pl.pallas_call(mixer_kernel, in_specs=[pl.BlockSpec(memory_space=pltpu.HB...  6.92 us
    unnamed x18, local copies, waits for them, and re-layouts  4.8 us
    all_to_all x1, starting transfers between devices, exchange(): return lax.all_to_all(x, 'ep', split_axis=0, concat_axis=0, tiled=True)  4.42 us
    pallas_call x1, Pallas kernels, run_expert(): pl.pallas_call(expert_kernel, in_specs=[in_vmem()] * 4, out_specs=pl.Bloc...  4.3 us
  transfers between devices with their start and end apart: 1, of which 1 were waited for; matrix products, arithmetic and copies ran while one was open for 0% of the time, Pallas kernels for 2%

profile of v6, /device:TPU:1, one launch (start us, length us, event | category | flops | bytes accessed | tf_op | source)
XLA Modules:
  0.0 90.1 jit_solution(15886335538620088253)
XLA Ops:
  0.6 0.0 copy-start.2
  0.6 6.9 %mixer.1 = (f32[64,4096]{1,0:T(8,128)}, f32[64,4096]{1,0:T(8,128)}, bf16[64,2048]{1,0:T(8,128)(2,1)S(1)}, bf16[64,2048]{1,0:T(8,128)(2,1)S(1)}, bf16[128,4,2048]{2,1,0:T(4,128)(2,1)S(1)}) custom-call(bf16[64,1024]{1,0:T(8,128)(2,1)} %refs_0_.1, f32[64,4096]{1,0:T(8,128)} %refs_1_.1, f32[64,4096]{1,0:T(8,128)} %refs_2_.1, f32[64,64]{1,0:T(8,128)} %refs_3_.1, ...), custom_call_target="tpu_custom_call" | custom-call | tf_op jit(solution)/shard_map/mixer/pallas_call | solution.py:259
  7.6 0.0 copy-start
  7.6 0.0 copy-start.1
  7.6 41.8 %all_to_all.10.y_ref = bf16[128,4,2048]{2,1,0:T(4,128)(2,1)S(1)} all-to-all(bf16[128,4,2048]{2,1,0:T(4,128)(2,1)S(1)} %get-tuple-element.10), channel_id=1, replica_groups=mesh['ep'=128] {'ep'}, dimensions={0} | all-to-all | bytes 4194304 | tf_op jit(solution)/shard_map/all_to_all | solution.py:407
  49.4 0.0 copy-done.2
  49.4 0.0 copy-done
  49.4 0.0 copy-done.1
  49.4 4.3 %expert.1 = bf16[128,4,2048]{2,1,0:T(4,128)(2,1)} custom-call(bf16[128,4,2048]{2,1,0:T(4,128)(2,1)S(1)} %all_to_all.10.y_ref, bf16[2048,512]{1,0:T(8,128)(2,1)S(1)} %bitcast.18, bf16[2048,512]{1,0:T(8,128)(2,1)S(1)} %bitcast.19, bf16[512,2048]{1,0:T(8,128)(2,1)S(1)} %bitcast.20), custom_call_target="tpu_custom_call" | custom-call | tf_op jit(solution)/shard_map/expert/pallas_call | solution.py:311
  53.7 0.0 copy-start.4
  53.7 0.0 copy-start.8
  53.7 4.4 %all-to-all-start.1 = ((bf16[128,4,2048]{2,1,0:T(4,128)(2,1)}), bf16[128,4,2048]{2,1,0:T(4,128)(2,1)S(1)}, u32[]{:S(2)}, u32[]{:S(2)}) async-start(bf16[128,4,2048]{2,1,0:T(4,128)(2,1)} %expert.1), calls=%async_computation.1 | async-start | bytes 4194304 | tf_op jit(solution)/shard_map/all_to_all | solution.py:407
  58.1 0.0 copy-done.4
  58.1 0.0 copy-done.8
  58.1 0.0 copy-start.5
  58.2 1.6 %copy-done.5 = bf16[2048,512]{1,0:T(8,128)(2,1)S(1)} copy-done((bf16[2048,512]{1,0:T(8,128)(2,1)S(1)}, bf16[2048,512]{1,0:T(8,128)(2,1)}, u32[]{:S(2)}) %copy-start.5) | copy-done | bytes 2097176
  59.7 0.0 copy-start.6
  59.7 1.6 %copy-done.6 = bf16[2048,512]{1,0:T(8,128)(2,1)S(1)} copy-done((bf16[2048,512]{1,0:T(8,128)(2,1)S(1)}, bf16[2048,512]{1,0:T(8,128)(2,1)}, u32[]{:S(2)}) %copy-start.6) | copy-done | bytes 2097176
  61.3 0.0 copy-start.7
  61.3 1.6 %copy-done.7 = bf16[512,2048]{1,0:T(8,128)(2,1)S(1)} copy-done((bf16[512,2048]{1,0:T(8,128)(2,1)S(1)}, bf16[512,2048]{1,0:T(8,128)(2,1)}, u32[]{:S(2)}) %copy-start.7) | copy-done | bytes 2097176
  62.9 0.0 copy-start.3
  62.9 1.7 %shared.1 = (f32[64,2048]{1,0:T(8,128)S(1)}, bf16[128,512]{1,0:T(8,128)(2,1)S(1)}) custom-call(bf16[64,2048]{1,0:T(8,128)(2,1)S(1)} %get-tuple-element.11.normed_ref, bf16[2048,512]{1,0:T(8,128)(2,1)S(1)} %copy-done.5, bf16[2048,512]{1,0:T(8,128)(2,1)S(1)} %copy-done.6, bf16[512,2048]{1,0:T(8,128)(2,1)S(1)} %copy-done.7, s32[6,64]{1,0:T(8,128)S(1)} %bitcast.23, ...), custom_call_target="tpu_custom_call" | custom-call | flops 8053063680 | bytes 8388608 | tf_op jit(solution)/shard_map/shared/pallas_call | solution.py:350
  64.6 24.1 %all-to-all-done.1.z_ref = bf16[128,4,2048]{2,1,0:T(4,128)(2,1)S(1)} async-done(((bf16[128,4,2048]{2,1,0:T(4,128)(2,1)}), bf16[128,4,2048]{2,1,0:T(4,128)(2,1)S(1)}, u32[]{:S(2)}, u32[]{:S(2)}) %all-to-all-start.1) | async-done | bytes 2097184 | tf_op jit(solution)/shard_map/all_to_all | solution.py:407
  88.7 0.0 copy-done.3
  88.7 1.3 %combine.1 = bf16[64,2048]{1,0:T(8,128)(2,1)} custom-call(bf16[128,4,2048]{2,1,0:T(4,128)(2,1)S(1)} %all-to-all-done.1.z_ref, bf16[128,512]{1,0:T(8,128)(2,1)S(1)} %get-tuple-element.12.mix_ref, f32[64,2048]{1,0:T(8,128)S(1)} %get-tuple-element.13.shared_ref, bf16[64,2048]{1,0:T(8,128)(2,1)S(1)} %get-tuple-element.14.mid_ref, f32[1,2048]{1,0:T(1,128)S(1)} %bitcast.21), custom_call_target="tpu_custom_call" | custom-call | tf_op jit(solution)/shard_map/combine/pallas_call | solution.py:377
Async XLA Ops:
  0.6 48.7 %copy-start.2 = (bf16[1,512,2048]{2,1,0:T(8,128)(2,1)S(1)}, bf16[1,512,2048]{2,1,0:T(8,128)(2,1)}, u32[]{:S(2)}) copy-start(bf16[1,512,2048]{2,1,0:T(8,128)(2,1)} %param.46) | copy-start | bytes 6291460
  7.6 41.8 %copy-start = (bf16[1,2048,512]{2,1,0:T(8,128)(2,1)S(1)}, bf16[1,2048,512]{2,1,0:T(8,128)(2,1)}, u32[]{:S(2)}) copy-start(bf16[1,2048,512]{2,1,0:T(8,128)(2,1)} %param.44) | copy-start | bytes 6291460
  7.6 41.8 %copy-start.1 = (bf16[1,2048,512]{2,1,0:T(8,128)(2,1)S(1)}, bf16[1,2048,512]{2,1,0:T(8,128)(2,1)}, u32[]{:S(2)}) copy-start(bf16[1,2048,512]{2,1,0:T(8,128)(2,1)} %param.45) | copy-start | bytes 6291460
  53.7 4.5 %copy-start.4 = (s32[64,6]{0,1:T(8,128)S(1)}, s32[64,6]{0,1:T(8,128)}, u32[]{:S(2)}) copy-start(s32[64,6]{0,1:T(8,128)} %param.42) | copy-start | bytes 4612
  53.7 4.5 %copy-start.8 = (f32[64,6]{0,1:T(8,128)S(1)}, f32[64,6]{0,1:T(8,128)}, u32[]{:S(2)}) copy-start(f32[64,6]{0,1:T(8,128)} %param.43) | copy-start | bytes 4612
  53.7 35.0 %all-to-all-start.1 = ((bf16[128,4,2048]{2,1,0:T(4,128)(2,1)}), bf16[128,4,2048]{2,1,0:T(4,128)(2,1)S(1)}, u32[]{:S(2)}, u32[]{:S(2)}) async-start(bf16[128,4,2048]{2,1,0:T(4,128)(2,1)} %expert.1), calls=%async_computation.1 | async-start | bytes 4194304 | tf_op jit(solution)/shard_map/all_to_all | solution.py:407
  58.1 1.6 %copy-start.5 = (bf16[2048,512]{1,0:T(8,128)(2,1)S(1)}, bf16[2048,512]{1,0:T(8,128)(2,1)}, u32[]{:S(2)}) copy-start(bf16[2048,512]{1,0:T(8,128)(2,1)} %wg_ref.1) | copy-start | bytes 6291460
  59.7 1.6 %copy-start.6 = (bf16[2048,512]{1,0:T(8,128)(2,1)S(1)}, bf16[2048,512]{1,0:T(8,128)(2,1)}, u32[]{:S(2)}) copy-start(bf16[2048,512]{1,0:T(8,128)(2,1)} %wu_ref.1) | copy-start | bytes 6291460
  61.3 1.6 %copy-start.7 = (bf16[512,2048]{1,0:T(8,128)(2,1)S(1)}, bf16[512,2048]{1,0:T(8,128)(2,1)}, u32[]{:S(2)}) copy-start(bf16[512,2048]{1,0:T(8,128)(2,1)} %wd_ref.1) | copy-start | bytes 6291460
  62.9 25.8 %copy-start.3 = (f32[2048]{0:T(1024)S(1)}, f32[2048]{0:T(1024)}, u32[]{:S(2)}) copy-start(f32[2048]{0:T(1024)} %param.41) | copy-start | bytes 24580

commit v7 on v6

--- a/solution.py
+++ b/solution.py
@@ -286,24 +286,17 @@
     )(*map(in_hbm, operands))
 
 
-def expert_kernel(y_ref, wg_ref, wu_ref, wd_ref, z_ref, h_ref, held, sems):
+def expert_kernel(y_ref, wg_ref, wu_ref, wd_ref, z_ref, h_ref):
     senders, slots, model = y_ref.shape
     x = y_ref[...].reshape(senders * slots, model)
     gate = dot(x, wg_ref[...])
     up = dot(x, wu_ref[...])
     h_ref[...] = (gate * jax.nn.sigmoid(gate) * up).astype(bf16)
-    pieces = sems.shape[0]
-    width = model // pieces
-    copies = []
-    for n in range(pieces):
-        out = dot(h_ref[...], wd_ref[:, width * n : width * (n + 1)]).astype(bf16)
-        held[:, :, width * n : width * (n + 1)] = out.reshape(senders, slots, width)
-        at = (slice(None), slice(None), pl.ds(width * n, width))
-        copy = pltpu.make_async_copy(held.at[at], z_ref.at[at], sems.at[n])
-        copy.start()
-        copies.append(copy)
-    for copy in copies:
-        copy.wait()
+    width = 512
+    for n in range(model // width):
+        at = slice(width * n, width * (n + 1))
+        out = dot(h_ref[...], wd_ref[:, at]).astype(bf16)
+        z_ref[:, :, at] = out.reshape(senders, slots, width)
 
 
 def run_expert(y, wg, wu, wd):
@@ -311,19 +304,15 @@
     return pl.pallas_call(
         expert_kernel,
         in_specs=[in_vmem()] * 4,
-        out_specs=pl.BlockSpec(memory_space=pltpu.HBM),
-        out_shape=pltpu.HBM(y.shape, bf16),
-        scratch_shapes=[
-            pltpu.VMEM((rows, wg.shape[1]), bf16),
-            pltpu.VMEM(y.shape, bf16),
-            pltpu.SemaphoreType.DMA((4,)),
-        ],
-        compiler_params=pltpu.CompilerParams(vmem_limit_bytes=20 << 20),
+        out_specs=in_vmem(),
+        out_shape=jax.ShapeDtypeStruct(y.shape, bf16),
+        scratch_shapes=[pltpu.VMEM((rows, wg.shape[1]), bf16)],
+        compiler_params=pltpu.CompilerParams(vmem_limit_bytes=16 << 20),
         name="expert",
     )(y, wg, wu, wd)
 
 
-def shared_kernel(normed_ref, wg_ref, wu_ref, wd_ref, routes_ref, weights_ref, out_ref, mix_ref):
+def shared_part(normed_ref, wg_ref, wu_ref, wd_ref, routes_ref, weights_ref, out_ref, mix_ref):
     x = normed_ref[...]
     gate = dot(x, wg_ref[...])
     up = dot(x, wu_ref[...])
@@ -345,25 +334,13 @@
         mix_ref[seq * h : seq * (h + 1), :] = jnp.where(hit, spread_rows(w), 0.0).T.astype(bf16)
 
 
-def run_shared(normed, wg, wu, wd, routes, weights):
-    seq, model = normed.shape
-    return pl.pallas_call(
-        shared_kernel,
-        out_shape=[
-            jax.ShapeDtypeStruct((seq, model), f32),
-            jax.ShapeDtypeStruct((2 * seq, EXPERTS * CAPACITY), bf16),
-        ],
-        in_specs=[in_vmem()] * 6,
-        out_specs=[in_vmem()] * 2,
-        compiler_params=pltpu.CompilerParams(vmem_limit_bytes=16 << 20),
-        cost_estimate=pl.CostEstimate(
-            flops=2 * seq * model * wg.shape[1] * 60, bytes_accessed=8 << 20, transcendentals=0
-        ),
-        name="shared",
-    )(normed, wg, wu, wd, routes, weights)
-
-
-def combine_kernel(z_ref, mix_ref, shared_ref, mid_ref, gain_ref, out_ref):
+def combine_kernel(
+    z_ref, normed_ref, sg_ref, su_ref, sd_ref, routes_ref, weights_ref, mid_ref, gain_ref,
+    out_ref, shared_ref, mix_ref,
+):
+    shared_part(
+        normed_ref, sg_ref, su_ref, sd_ref, routes_ref, weights_ref, shared_ref, mix_ref
+    )
     seq = mid_ref.shape[0]
     both = dot(mix_ref[...], z_ref[...].reshape(mix_ref.shape[1], out_ref.shape[1]))
     routed = both[:seq] + both[seq:]
@@ -373,15 +350,19 @@
     ).astype(bf16)
 
 
-def run_combine(z, mix, shared, mid, gain):
+def run_combine(z, normed, sg, su, sd, routes, weights, mid, gain):
     return pl.pallas_call(
         combine_kernel,
+        in_specs=[in_vmem()] * 9,
+        out_specs=in_vmem(),
         out_shape=jax.ShapeDtypeStruct(mid.shape, bf16),
-        in_specs=[in_vmem()] * 5,
-        out_specs=in_vmem(),
+        scratch_shapes=[
+            pltpu.VMEM(mid.shape, f32),
+            pltpu.VMEM((2 * mid.shape[0], EXPERTS * CAPACITY), bf16),
+        ],
         compiler_params=pltpu.CompilerParams(vmem_limit_bytes=16 << 20),
         name="combine",
-    )(z, mix, shared, mid, gain)
+    )(z, normed, sg, su, sd, routes, weights, mid, gain)
 
 
 def per_device(
@@ -407,9 +388,11 @@
         return lax.all_to_all(x, "ep", split_axis=0, concat_axis=0, tiled=True)
 
     arrived = exchange(outgoing)
-    shared, mix = run_shared(normed, shared_gate, shared_up, shared_down, routes_t, weights_t)
     returned = exchange(run_expert(arrived, expert_gate[0], expert_up[0], expert_down[0]))
-    layer_out = run_combine(returned, mix, shared, mid, row(moe_out_gain))
+    layer_out = run_combine(
+        returned, normed, shared_gate, shared_up, shared_down, routes_t, weights_t, mid,
+        row(moe_out_gain),
+    )
     return layer_out, next_real, next_imag
 
 

time: 90.4 us -> 90.5 us (level)
  blocking collectives: 41.8 us -> 76.4 us
  waiting for transfers between devices: 24.1 us -> 0 us
  local copies, waits for them, and re-layouts: 4.8 us -> 0.05 us
  starting transfers between devices: 4.42 us -> 0 us
  Pallas kernels: 14.2 us -> 13.2 us
    all_to_all x1 -> x2, blocking collectives: 41.8 us -> 76.4 us  [exchange(): return lax.all_to_all(x, 'ep', split_axis=0, concat_axis=0, tiled=True)]
    all_to_all x1 -> x0, waiting for transfers between devices: 24.1 us -> none  [exchange(): return lax.all_to_all(x, 'ep', split_axis=0, concat_axis=0, tiled=True)]
    unnamed x18, local copies, waits for them, and re-layouts: 4.8 us -> 0.05 us
    all_to_all x1 -> x0, starting transfers between devices: 4.42 us -> none  [exchange(): return lax.all_to_all(x, 'ep', split_axis=0, concat_axis=0, tiled=True)]
    pallas_call x3 -> x2, Pallas kernels: 7.33 us -> 6.33 us  [the longest x1 3.42 us: run_expert(): pl.pallas_call(expert_kernel, in_specs=[in_vmem()] * 4, out_specs=in_vmem...]
  transfers between devices with their start and end apart: 1 -> 0, of which waited for: 1 -> 0; matrix products, arithmetic and copies ran while one was open for 0% -> 0% of each run, Pallas kernels for 2% -> 0%
where the time goes in v7:
time: 90.5 us; the launch traced here: 90.4 us
  blocking collectives  76.4 us (84%)
  Pallas kernels  13.2 us (15%)
    all_to_all x2, blocking collectives, exchange(): return lax.all_to_all(x, 'ep', split_axis=0, concat_axis=0, tiled=True)  76.4 us
    pallas_call x1, Pallas kernels, run_mixer(): pl.pallas_call(mixer_kernel, in_specs=[pl.BlockSpec(memory_space=pltpu.HB...  6.92 us
    pallas_call x1, Pallas kernels, run_expert(): pl.pallas_call(expert_kernel, in_specs=[in_vmem()] * 4, out_specs=in_vmem...  3.42 us
    pallas_call x1, Pallas kernels, run_combine(): pl.pallas_call(combine_kernel, in_specs=[in_vmem()] * 9, out_specs=in_vme...  2.91 us

profile of v7, /device:TPU:1, one launch (start us, length us, event | category | flops | bytes accessed | tf_op | source)
XLA Modules:
  0.0 90.4 jit_solution(3761961581100146191)
XLA Ops:
  0.6 0.0 copy-start.2
  0.6 6.9 %mixer.1 = (f32[64,4096]{1,0:T(8,128)}, f32[64,4096]{1,0:T(8,128)}, bf16[64,2048]{1,0:T(8,128)(2,1)S(1)}, bf16[64,2048]{1,0:T(8,128)(2,1)S(1)}, bf16[128,4,2048]{2,1,0:T(4,128)(2,1)S(1)}) custom-call(bf16[64,1024]{1,0:T(8,128)(2,1)} %refs_0_.1, f32[64,4096]{1,0:T(8,128)} %refs_1_.1, f32[64,4096]{1,0:T(8,128)} %refs_2_.1, f32[64,64]{1,0:T(8,128)} %refs_3_.1, ...), custom_call_target="tpu_custom_call" | custom-call | tf_op jit(solution)/shard_map/mixer/pallas_call | solution.py:259
  7.6 0.0 copy-start
  7.6 0.0 copy-start.1
  7.6 41.8 %all_to_all.10.y_ref = bf16[128,4,2048]{2,1,0:T(4,128)(2,1)S(1)} all-to-all(bf16[128,4,2048]{2,1,0:T(4,128)(2,1)S(1)} %get-tuple-element.8), channel_id=1, replica_groups=mesh['ep'=128] {'ep'}, dimensions={0} | all-to-all | bytes 4194304 | tf_op jit(solution)/shard_map/all_to_all | solution.py:388
  49.4 0.0 copy-done.2
  49.4 0.0 copy-done
  49.4 0.0 copy-done.1
  49.4 0.0 copy-start.5
  49.4 0.0 copy-start.7
  49.4 0.0 copy-start.8
  49.4 3.4 %expert.1 = bf16[128,4,2048]{2,1,0:T(4,128)(2,1)S(1)} custom-call(bf16[128,4,2048]{2,1,0:T(4,128)(2,1)S(1)} %all_to_all.10.y_ref, bf16[2048,512]{1,0:T(8,128)(2,1)S(1)} %bitcast.18, bf16[2048,512]{1,0:T(8,128)(2,1)S(1)} %bitcast.19, bf16[512,2048]{1,0:T(8,128)(2,1)S(1)} %bitcast.20), custom_call_target="tpu_custom_call" | custom-call | tf_op jit(solution)/shard_map/expert/pallas_call | solution.py:304
  52.8 0.0 copy-start.3
  52.8 0.0 copy-start.4
  52.9 0.0 copy-start.6
  52.9 34.6 %all_to_all.11.z_ref = bf16[128,4,2048]{2,1,0:T(4,128)(2,1)S(1)} all-to-all(bf16[128,4,2048]{2,1,0:T(4,128)(2,1)S(1)} %expert.1), channel_id=1, replica_groups=mesh['ep'=128] {'ep'}, dimensions={0} | all-to-all | bytes 4194304 | tf_op jit(solution)/shard_map/all_to_all | solution.py:388
  87.5 0.0 copy-done.5
  87.5 0.0 copy-done.7
  87.5 0.0 copy-done.8
  87.5 0.0 copy-done.3
  87.5 0.0 copy-done.4
  87.5 0.0 copy-done.6
  87.5 2.9 %combine.1 = bf16[64,2048]{1,0:T(8,128)(2,1)} custom-call(bf16[128,4,2048]{2,1,0:T(4,128)(2,1)S(1)} %all_to_all.11.z_ref, bf16[64,2048]{1,0:T(8,128)(2,1)S(1)} %get-tuple-element.9.normed_ref, bf16[2048,512]{1,0:T(8,128)(2,1)S(1)} %copy-done.3, bf16[2048,512]{1,0:T(8,128)(2,1)S(1)} %copy-done.4, bf16[512,2048]{1,0:T(8,128)(2,1)S(1)} %copy-done.5, ...), custom_call_target="tpu_custom_call" | custom-call | tf_op jit(solution)/shard_map/combine/pallas_call | solution.py:354
Async XLA Ops:
  0.6 48.7 %copy-start.2 = (bf16[1,512,2048]{2,1,0:T(8,128)(2,1)S(1)}, bf16[1,512,2048]{2,1,0:T(8,128)(2,1)}, u32[]{:S(2)}) copy-start(bf16[1,512,2048]{2,1,0:T(8,128)(2,1)} %param.46) | copy-start | bytes 6291460
  7.6 41.8 %copy-start = (bf16[1,2048,512]{2,1,0:T(8,128)(2,1)S(1)}, bf16[1,2048,512]{2,1,0:T(8,128)(2,1)}, u32[]{:S(2)}) copy-start(bf16[1,2048,512]{2,1,0:T(8,128)(2,1)} %param.44) | copy-start | bytes 6291460
  7.6 41.8 %copy-start.1 = (bf16[1,2048,512]{2,1,0:T(8,128)(2,1)S(1)}, bf16[1,2048,512]{2,1,0:T(8,128)(2,1)}, u32[]{:S(2)}) copy-start(bf16[1,2048,512]{2,1,0:T(8,128)(2,1)} %param.45) | copy-start | bytes 6291460
  49.4 38.1 %copy-start.5 = (bf16[512,2048]{1,0:T(8,128)(2,1)S(1)}, bf16[512,2048]{1,0:T(8,128)(2,1)}, u32[]{:S(2)}) copy-start(bf16[512,2048]{1,0:T(8,128)(2,1)} %sd_ref.1) | copy-start | bytes 6291460
  49.4 38.1 %copy-start.7 = (f32[2048]{0:T(1024)S(1)}, f32[2048]{0:T(1024)}, u32[]{:S(2)}) copy-start(f32[2048]{0:T(1024)} %param.41) | copy-start | bytes 24580
  49.4 38.1 %copy-start.8 = (f32[64,6]{0,1:T(8,128)S(1)}, f32[64,6]{0,1:T(8,128)}, u32[]{:S(2)}) copy-start(f32[64,6]{0,1:T(8,128)} %param.43) | copy-start | bytes 4612
  52.8 34.7 %copy-start.3 = (bf16[2048,512]{1,0:T(8,128)(2,1)S(1)}, bf16[2048,512]{1,0:T(8,128)(2,1)}, u32[]{:S(2)}) copy-start(bf16[2048,512]{1,0:T(8,128)(2,1)} %sg_ref.1) | copy-start | bytes 6291460
  52.8 34.7 %copy-start.4 = (bf16[2048,512]{1,0:T(8,128)(2,1)S(1)}, bf16[2048,512]{1,0:T(8,128)(2,1)}, u32[]{:S(2)}) copy-start(bf16[2048,512]{1,0:T(8,128)(2,1)} %su_ref.1) | copy-start | bytes 6291460
  52.9 34.7 %copy-start.6 = (s32[64,6]{0,1:T(8,128)S(1)}, s32[64,6]{0,1:T(8,128)}, u32[]{:S(2)}) copy-start(s32[64,6]{0,1:T(8,128)} %param.42) | copy-start | bytes 4612
